TPU v7x, 32 devices: a whole 2x2x4 slice. The times are simulated.
32 devices in a mesh: gr: 2 (over x), sp: 8 (over z, y), tp: 2 (over core).
Axes of the slice: x: 2, y: 2, z: 4, core: 2. Of those that a mesh axis runs over, the one named last changes fastest.
Arguments:
- tokens: bfloat16 [2, 2, 6144, 2048], P('gr', 'tp', 'sp'), may hold values from -6 to 6
- key_weight: bfloat16 [2048, 2048], replicated, may hold values from -0.125 to 0.125
- value_weight: bfloat16 [2048, 2048], replicated, may hold values from -0.125 to 0.125
- cum_gate: float32 [2, 32, 2, 6144], P('gr', None, 'tp', 'sp'), may hold values from -12588 to 0, as said below
- query: bfloat16 [2, 32, 64], P('gr', 'sp'), may hold values from -12 to 12
Outputs:
- kv_cache: bfloat16 [2, 32, 12288, 128], P('gr', 'sp', 'tp')
- gate_cache: float32 [2, 32, 12288], P('gr', 'sp', 'tp')
- read: bfloat16 [2, 32, 64], P('gr', 'sp')
Inputs may be any that keep to these rules, and one draw needn't show every extreme that they name: `cum_gate`: each head's entries never rise along the positions.
All inputs are finite; a program needn't handle non-finite values.
Results may differ from a plain program's by a relative error of at most 0.012.
Values may be sent and summed in bfloat16 or wider, within the bound.
No kernel may reach another device: no remote copies, remote signals or barrier semaphores. Data moves between devices by JAX's collectives and lax.ppermute only.
A program may use at most 128 MiB of HBM per device.

v0:
```python
import functools

import jax
import jax.numpy as jnp
from jax import lax
from jax.experimental import pallas as pl
from jax.experimental.pallas import tpu as pltpu
from jax.sharding import PartitionSpec as P

LANES = 128
ROWS = 64
TAIL = 192
MIB = 1 << 20


def owned(columns, owner, width):
    sharers = columns.shape[1] // width
    mine = columns[:, :width]
    for at in range(1, sharers):
        mine = jnp.where(owner % sharers == at, columns[:, at * width : (at + 1) * width], mine)
    return mine


def project_block(step, me_ref, tokens_ref, key_ref, value_ref, out_ref):
    heads, _, width = out_ref.shape
    size = width // 2
    owner = me_ref[0] ^ step
    rows = tokens_ref[...]
    keys = jnp.dot(rows, key_ref[...], preferred_element_type=jnp.float32)
    values = jnp.dot(rows, value_ref[...], preferred_element_type=jnp.float32)
    keys = owned(keys, owner, heads * size).astype(out_ref.dtype)
    values = owned(values, owner, heads * size).astype(out_ref.dtype)
    for head in range(heads):
        part = slice(head * size, (head + 1) * size)
        out_ref[head] = jnp.concatenate([keys[:, part], values[:, part]], axis=-1)


def project(me, step, rows, count, key_weight, value_weight, heads, size):
    width = rows.shape[1]
    tiles = 2 if count % 32 == 0 else 1
    tile = count // tiles
    columns = max(heads * size, LANES)
    sharers = columns // (heads * size)

    def weight_index(i, s):
        return (0, (s[0] ^ step) // sharers)

    return pl.pallas_call(
        functools.partial(project_block, step),
        grid_spec=pltpu.PrefetchScalarGridSpec(
            num_scalar_prefetch=1,
            grid=(tiles,),
            in_specs=[
                pl.BlockSpec((tile, width), lambda i, s: (i, 0)),
                pl.BlockSpec((width, columns), weight_index),
                pl.BlockSpec((width, columns), weight_index),
            ],
            out_specs=pl.BlockSpec((heads, tile, 2 * size), lambda i, s: (0, i, 0)),
        ),
        out_shape=jax.ShapeDtypeStruct((heads, count, 2 * size), rows.dtype),
        cost_estimate=pl.CostEstimate(
            flops=4 * count * width * columns,
            bytes_accessed=2 * (count * width + 2 * width * columns + 2 * count * columns),
            transcendentals=0,
        ),
        name="project",
    )(me, rows, key_weight, value_weight)


def place_block(parts, length, block_ref, *refs):
    out_ref, left = refs[-2:]
    me = lax.axis_index("sp")
    writes = []
    for step, there, here, count in parts:
        start = pl.multiple_of((me ^ step) * length + there, ROWS)
        taken, put = block_ref.at[:, pl.ds(here, count), :], out_ref.at[:, pl.ds(start, count), :]
        writes.append(pltpu.make_async_copy(taken, put, left.at[len(writes)]))
    for write in writes:
        write.start()
    for write in writes:
        write.wait()


def place(cache, block, parts, places, length):
    heads, _, width = block.shape
    anywhere = pl.BlockSpec(memory_space=pl.ANY)
    old = () if cache is None else (cache,)
    return pl.pallas_call(
        functools.partial(place_block, parts, length),
        in_specs=[pl.BlockSpec(memory_space=pltpu.VMEM)] + [anywhere] * len(old),
        out_specs=anywhere,
        out_shape=jax.ShapeDtypeStruct((heads, places * length, width), block.dtype),
        scratch_shapes=[pltpu.SemaphoreType.DMA((len(parts),))],
        input_output_aliases={1: 0} if old else {},
        cost_estimate=pl.CostEstimate(flops=block.size, bytes_accessed=4 * block.size, transcendentals=0),
        compiler_params=pltpu.CompilerParams(vmem_limit_bytes=4 * MIB),
        name="place",
    )(block, *old)


def read_blocks(steps, near, me_ref, query_ref, gates_ref, borrowed_ref, *refs):
    block_refs, out_ref = refs[:-1], refs[-1]
    heads, _, width = block_refs[0].shape
    size = width // 2
    lanes = lax.broadcasted_iota(jnp.int32, (1, width), 1)
    for step, block_ref in zip(steps, block_refs):
        owner = me_ref[0] ^ step
        rows = block_ref.shape[1]
        for head in range(heads):
            block = block_ref[head]
            query = jnp.broadcast_to(query_ref[owner, pl.ds(head, 1), :], (8, width)).astype(block.dtype)
            scores = lax.dot_general(query, block, (((1,), (1,)), ((), ())), preferred_element_type=jnp.float32)
            gates = gates_ref[owner, pl.ds(head, 1), :]
            if step < near:
                more = borrowed_ref[lax.rem(owner, near), pl.ds(head, 1), :]
                gates = jnp.concatenate([gates, more], axis=-1)
            scores = scores[0:1] * size ** (-0.5) - gates[:, :rows]
            top = jnp.max(scores, axis=-1, keepdims=True)
            weights = jnp.exp(scores - top)
            total = jnp.sum(weights, axis=-1, keepdims=True)
            probs = jnp.broadcast_to(weights, (8, rows)).astype(block.dtype)
            weighted = jnp.dot(probs, block, preferred_element_type=jnp.float32)[0:1]
            row = jnp.where(lanes == 0, top, jnp.where(lanes == 1, total, weighted))
            out_ref[owner, pl.ds(head, 1), :] = row


def partial_reads(me, steps, near, queries, gates, borrowed, blocks):
    places, heads, size = queries.shape
    rows = gates.shape[2]
    queries = jnp.pad(queries.astype(jnp.float32), ((0, 0), (0, 0), (0, size)))
    whole = pl.BlockSpec(memory_space=pltpu.VMEM)
    return pl.pallas_call(
        functools.partial(read_blocks, steps, near),
        in_specs=[pl.BlockSpec(memory_space=pltpu.SMEM)] + [whole] * (3 + len(blocks)),
        out_specs=whole,
        out_shape=jax.ShapeDtypeStruct((places, heads, 2 * size), jnp.float32),
        cost_estimate=pl.CostEstimate(
            flops=16 * places * heads * rows * 2 * size,
            bytes_accessed=2 * places * heads * rows * 2 * size,
            transcendentals=places * heads * rows,
        ),
        name="read",
    )(me, queries, gates, borrowed, *blocks)


def merged_reads(parts, size):
    tops = parts[:, :, 0:1]
    top = jnp.max(tops, axis=0, keepdims=True)
    scale = jnp.exp(tops - top)
    total = jnp.sum(parts[:, :, 1:2] * scale, axis=0)
    weighted = jnp.sum(parts[:, :, size:] * scale, axis=0)
    return weighted / total


def packed_gates(gates):
    places, heads, length = gates.shape
    groups = gates.reshape(places, heads, length // LANES, LANES)
    first = groups[..., :1]
    falls = (groups - first).astype(jnp.bfloat16).reshape(gates.shape)
    rest, terms = first[..., 0], []
    for _ in range(3):
        terms.append(lax.reduce_precision(rest, 8, 7))
        rest = rest - terms[-1]
    return jnp.concatenate([falls] + [term.astype(jnp.bfloat16) for term in terms], axis=-1)


def unpacked_gates(packed, length):
    places, heads, _ = packed.shape
    packed = packed.astype(jnp.float32)
    falls, terms = packed[..., :length], packed[..., length:]
    first = jnp.sum(terms.reshape(places, heads, 3, length // LANES), axis=2)
    groups = falls.reshape(places, heads, length // LANES, LANES) + first[..., None]
    return groups.reshape(places, heads, length)


def plan(places):
    far = places // 2
    across, near = list(range(far, places)), list(range(1, far))
    half = len(across) // 2
    order = across[half:][::-1] + near + across[:half]
    return order[:-1], order[-1:]


def on_device(places, tokens, key_weight, value_weight, cum_gate, query):
    heads, size = query.shape[1:]
    rows = tokens[0, 0]
    length = rows.shape[0]
    far = places // 2
    me = lax.axis_index("sp").astype(jnp.int32)
    here = me.reshape(1)
    early, late = plan(places)
    kept = length - ROWS

    def swap(value, step):
        return lax.ppermute(value, "sp", [(i, i ^ step) for i in range(places)])

    def exchange(value):
        return lax.all_to_all(value, "sp", split_axis=0, concat_axis=0, tiled=True)

    lent = swap(rows[kept:], far)
    more = jnp.concatenate([rows, lent], axis=0)

    def block_of(step):
        mine, count = (more, length + ROWS) if step < far else (rows, kept)
        return project(here, step, mine, count, key_weight, value_weight, heads, size)

    def parts_of(step):
        if step < far:
            return ((step, 0, 0, length), (step ^ far, kept, length, ROWS))
        return ((step, 0, 0, kept),)

    sent, arrived = {}, []
    for step in early + late:
        sent[step] = block_of(step)
        pieces = [("", sent[step], parts_of(step))]
        if step in late:
            head = kept - TAIL
            pieces = [
                ("", sent[step][:, :head], ((step, 0, 0, head),)),
                ("_tail", sent[step][:, head:], ((step, head, 0, TAIL),)),
            ]
        for name, block, parts in pieces:
            arrived.append((f"place_{step}{name}", swap(block, step), parts))

    gates = cum_gate[0, :, 0, :].reshape(places, heads, length)
    asked = jnp.broadcast_to(query, (places, heads, size))
    told = exchange(jnp.concatenate([packed_gates(gates), asked], axis=-1))
    queries = told[:, :, -size:]
    gate_parts = unpacked_gates(told[:, :, :-size], length)
    gate_cache = jnp.transpose(gate_parts, (1, 0, 2)).reshape(1, heads, places * length)
    borrowed = swap(lax.dynamic_slice(gates, ((me ^ far) & far, 0, kept), (far, heads, ROWS)), far)

    sent[0] = block_of(0)
    cache = place(None, sent[0], parts_of(0), places, length)
    steps = [0] + early + late
    parts = partial_reads(here, steps, far, queries, gates, borrowed, [sent[step] for step in steps])
    parts = exchange(parts)
    parts = lax.all_gather(parts, "tp", tiled=True)
    read = merged_reads(parts, size).astype(jnp.bfloat16)[None]

    for name, block, parts in arrived:
        if name == f"place_{late[-1]}":
            cache, read = lax.optimization_barrier((cache, read))
        cache = place(cache, block, parts, places, length)
    return (cache[None], gate_cache, read)


def solution(mesh):
    placed = (P("gr", "tp", "sp", None), P(), P(), P("gr", None, "tp", "sp"), P("gr", "sp", None))
    places = mesh.shape["sp"]

    def body(*args):
        return on_device(places, *args)

    return jax.shard_map(
        body,
        mesh=mesh,
        in_specs=placed,
        out_specs=(P("gr", "sp", "tp", None), P("gr", "sp", "tp"), P("gr", "sp", None)),
        check_vma=False,
    )
```

profile of v0, /device:TPU:0, one launch (start us, length us, event | category | flops | bytes accessed | tf_op | source)
XLA Modules:
  0.0 175.9 jit_solution(15256418640100226172)
XLA Ops:
  0.6 1.1 reduce.2
  3.8 7.3 %all-to-all-start = ((bf16[8,4,850]{2,1,0:T(4,128)(2,1)}), bf16[8,4,850]{2,1,0:T(4,128)(2,1)S(1)}, u32[]{:S(2)}, u32[]{:S(2)}) async-start(bf16[8,4,850]{2,1,0:T(4,128)(2,1)} %concatenate.7), calls=%async_computation | async-start | bytes 114688 | tf_op jit(solution)/shard_map/all_to_all | solution.py:198
  11.1 1.0 slice_bitcast_fusion
  12.1 3.0 %collective-permute-start.3 = (bf16[64,2048]{1,0:T(8,128)(2,1)S(1)}, bf16[64,2048]{1,0:T(8,128)(2,1)S(1)}, u32[]{:S(2)}, u32[]{:S(2)}) collective-permute-start(bf16[64,2048]{1,0:T(8,128)(2,1)S(1)} %slice_bitcast_fusion), channel_id=1, source_target_pairs={{0,8},{2,10},{4,12},{6,14},{8,0},{10,2},{12,4},{14,6},{1,9},{3,11}... | collective-permute-start | bytes 786440 | tf_op jit(solution)/shard_map/ppermute | solution.py:195
  15.2 4.7 %project.14.refs_1_ = bf16[4,704,128]{2,1,0:T(8,128)(2,1)} custom-call(s32[1]{0:T(128)} %bitcast.me_ref, bf16[768,2048]{1,0:T(8,128)(2,1)} %bitcast.26, bf16[2048,2048]{1,0:T(8,128)(2,1)} %key_ref.15, bf16[2048,2048]{1,0:T(8,128)(2,1)} %value_ref.15), custom_call_target="tpu_custom_call" | custom-call | flops 1476395008 | bytes 5701632 | tf_op jit(solution)/shard_map/project/pallas_call | solution.py:48
  19.9 4.7 %collective-permute-start.8 = (bf16[4,704,128]{2,1,0:T(8,128)(2,1)}, bf16[4,704,128]{2,1,0:T(8,128)(2,1)S(1)}, u32[]{:S(2)}, u32[]{:S(2)}) collective-permute-start(bf16[4,704,128]{2,1,0:T(8,128)(2,1)} %project.14.refs_1_), channel_id=1, source_target_pairs={{0,14},{2,12},{4,10},{6,8},{8,6},{10,4},{12,2},{14,0},{1,15},{3,13... | collective-permute-start | bytes 2162696 | tf_op jit(solution)/shard_map/ppermute | solution.py:195
  24.6 4.8 %project.13.refs_2_ = bf16[4,704,128]{2,1,0:T(8,128)(2,1)} custom-call(s32[1]{0:T(128)} %bitcast.me_ref, bf16[768,2048]{1,0:T(8,128)(2,1)} %bitcast.27, bf16[2048,2048]{1,0:T(8,128)(2,1)} %key_ref.15, bf16[2048,2048]{1,0:T(8,128)(2,1)} %value_ref.15), custom_call_target="tpu_custom_call" | custom-call | flops 1476395008 | bytes 5701632 | tf_op jit(solution)/shard_map/project/pallas_call | solution.py:48
  29.9 4.8 %project.9.refs_6_ = bf16[4,704,128]{2,1,0:T(8,128)(2,1)} custom-call(s32[1]{0:T(128)} %bitcast.me_ref, bf16[768,2048]{1,0:T(8,128)(2,1)} %bitcast.28, bf16[2048,2048]{1,0:T(8,128)(2,1)} %key_ref.15, bf16[2048,2048]{1,0:T(8,128)(2,1)} %value_ref.15), custom_call_target="tpu_custom_call" | custom-call | flops 1476395008 | bytes 5701632 | tf_op jit(solution)/shard_map/project/pallas_call | solution.py:48
  35.2 4.8 %project.8.refs_7_ = bf16[4,704,128]{2,1,0:T(8,128)(2,1)} custom-call(s32[1]{0:T(128)} %bitcast.me_ref, bf16[768,2048]{1,0:T(8,128)(2,1)} %bitcast.29, bf16[2048,2048]{1,0:T(8,128)(2,1)} %key_ref.15, bf16[2048,2048]{1,0:T(8,128)(2,1)} %value_ref.15), custom_call_target="tpu_custom_call" | custom-call | flops 1476395008 | bytes 5701632 | tf_op jit(solution)/shard_map/project/pallas_call | solution.py:48
  40.0 1.9 %slice.49 = bf16[4,512,128]{2,1,0:T(8,128)(2,1)} slice(bf16[4,704,128]{2,1,0:T(8,128)(2,1)} %project.8.refs_7_), slice={[0:4], [0:512], [0:128]} | slice | bytes 1048576 | tf_op jit(solution)/shard_map/slice | solution.py:219
  41.9 1.6 slice.48
  45.2 29.3 %collective-permute-done.3 = bf16[64,2048]{1,0:T(8,128)(2,1)S(1)} collective-permute-done((bf16[64,2048]{1,0:T(8,128)(2,1)S(1)}, bf16[64,2048]{1,0:T(8,128)(2,1)S(1)}, u32[]{:S(2)}, u32[]{:S(2)}) %collective-permute-start.3) | collective-permute-done | bytes 262176 | tf_op jit(solution)/shard_map/ppermute | solution.py:195
  74.5 4.1 %pad_maximum_fusion.tokens_ref = bf16[832,2048]{1,0:T(8,128)(2,1)} fusion(bf16[64,2048]{1,0:T(8,128)(2,1)S(1)} %collective-permute-done.3, bf16[768,2048]{1,0:T(8,128)(2,1)} %bitcast.30), kind=kLoop, calls=%fused_computation | loop fusion | flops 6815744 | bytes 6815744 | tf_op jit(solution)/shard_map/concatenate | solution.py:201
  78.6 5.1 %project.12.refs_3_ = bf16[4,832,128]{2,1,0:T(8,128)(2,1)} custom-call(s32[1]{0:T(128)} %bitcast.me_ref, bf16[832,2048]{1,0:T(8,128)(2,1)} %pad_maximum_fusion.tokens_ref, bf16[2048,2048]{1,0:T(8,128)(2,1)} %key_ref.15, bf16[2048,2048]{1,0:T(8,128)(2,1)} %value_ref.15), custom_call_target="tpu_custom_call" | custom-call | flops 1744830464 | bytes 6356992 | tf_op jit(solution)/shard_map/project/pallas_call | solution.py:48
  83.7 1.5 collective-permute-start.6
  85.2 5.1 %project.10.refs_5_ = bf16[4,832,128]{2,1,0:T(8,128)(2,1)} custom-call(s32[1]{0:T(128)} %bitcast.me_ref, bf16[832,2048]{1,0:T(8,128)(2,1)} %pad_maximum_fusion.tokens_ref, bf16[2048,2048]{1,0:T(8,128)(2,1)} %key_ref.15, bf16[2048,2048]{1,0:T(8,128)(2,1)} %value_ref.15), custom_call_target="tpu_custom_call" | custom-call | flops 1744830464 | bytes 6356992 | tf_op jit(solution)/shard_map/project/pallas_call | solution.py:48
  90.3 5.1 %project.11.refs_4_ = bf16[4,832,128]{2,1,0:T(8,128)(2,1)} custom-call(s32[1]{0:T(128)} %bitcast.me_ref, bf16[832,2048]{1,0:T(8,128)(2,1)} %pad_maximum_fusion.tokens_ref, bf16[2048,2048]{1,0:T(8,128)(2,1)} %key_ref.15, bf16[2048,2048]{1,0:T(8,128)(2,1)} %value_ref.15), custom_call_target="tpu_custom_call" | custom-call | flops 1744830464 | bytes 6356992 | tf_op jit(solution)/shard_map/project/pallas_call | solution.py:48
  95.4 5.2 %project.15.block_ref.refs_0_ = bf16[4,832,128]{2,1,0:T(8,128)(2,1)} custom-call(s32[1]{0:T(128)} %bitcast.me_ref, bf16[832,2048]{1,0:T(8,128)(2,1)} %pad_maximum_fusion.tokens_ref, bf16[2048,2048]{1,0:T(8,128)(2,1)} %key_ref.15, bf16[2048,2048]{1,0:T(8,128)(2,1)} %value_ref.15), custom_call_target="tpu_custom_call" | custom-call | flops 1744830464 | bytes 6356992 | tf_op jit(solution)/shard_map/project/pallas_call | solution.py:48
  101.2 13.1 %read.1 = f32[8,4,128]{2,1,0:T(4,128)} custom-call(s32[1]{0:T(128)} %bitcast.me_ref, f32[8,4,128]{2,1,0:T(4,128)} %pad_convert_fusion.query_ref, f32[8,4,768]{2,1,0:T(4,128)} %copy-done.3, f32[4,4,64]{2,1,0:T(4,128)} %copy-done.5, bf16[4,832,128]{2,1,0:T(8,128)(2,1)} %project.15.block_ref.refs_0_, bf16[4,704,128]{2,1,0:T(8,128)(2,1)} %project.14.refs_1_, ...), custom_call_target="tpu_custom_call" | custom-call | flops 50331648 | bytes 6291456 | tf_op jit(solution)/shard_map/read/pallas_call | solution.py:132
  114.3 3.4 %all-to-all-start.1 = ((f32[8,4,128]{2,1,0:T(4,128)}), f32[8,4,128]{2,1,0:T(4,128)S(1)}, u32[]{:S(2)}, u32[]{:S(2)}) async-start(f32[8,4,128]{2,1,0:T(4,128)} %read.1), calls=%async_computation.1 | async-start | bytes 32768 | tf_op jit(solution)/shard_map/all_to_all | solution.py:198
  118.5 2.9 %collective-permute-start.4 = (bf16[4,832,128]{2,1,0:T(8,128)(2,1)}, bf16[4,832,128]{2,1,0:T(8,128)(2,1)S(1)}, u32[]{:S(2)}, u32[]{:S(2)}) collective-permute-start(bf16[4,832,128]{2,1,0:T(8,128)(2,1)} %project.10.refs_5_), channel_id=1, source_target_pairs={{0,6},{2,4},{4,2},{6,0},{8,14},{10,12},{12,10},{14,8},{1,7},{3,5},... | collective-permute-start | bytes 2555912 | tf_op jit(solution)/shard_map/ppermute | solution.py:195
  121.5 1.6 slice_add_fusion
  124.0 14.4 %all-to-all-done.1 = f32[8,4,128]{2,1,0:T(4,128)S(1)} async-done(((f32[8,4,128]{2,1,0:T(4,128)}), f32[8,4,128]{2,1,0:T(4,128)S(1)}, u32[]{:S(2)}, u32[]{:S(2)}) %all-to-all-start.1) | async-done | bytes 16416 | tf_op jit(solution)/shard_map/all_to_all | solution.py:198
  138.4 1.8 %all_gather.3 = f32[16,4,128]{2,1,0:T(4,128)S(1)} all-gather(f32[8,4,128]{2,1,0:T(4,128)S(1)} %all-to-all-done.1), channel_id=1, replica_groups=mesh['gr'=2,'sp'=8,'tp'=2] {'tp'}, dimensions={0}, use_global_device_ids=true | all-gather | bytes 49152 | tf_op jit(solution)/shard_map/all_gather | solution.py:238
  141.1 1.1 copy-done.2
  143.2 2.0 %place.11.refs_0_ = bf16[4,6144,128]{2,1,0:T(8,128)(2,1)} custom-call(bf16[4,704,128]{2,1,0:T(8,128)(2,1)} %collective-permute-done.7.block_ref, bf16[4,6144,128]{2,1,0:T(8,128)(2,1)} %place.10.refs_0_), custom_call_target="tpu_custom_call", output_to_operand_aliasing={{}: (1, {})} | custom-call | flops 360448 | bytes 1441792 | tf_op jit(solution)/shard_map/place/pallas_call | solution.py:88
  145.2 3.7 %collective-permute-start = (bf16[4,192,128]{2,1,0:T(8,128)(2,1)S(1)}, bf16[4,192,128]{2,1,0:T(8,128)(2,1)S(1)}, u32[]{:S(2)}, u32[]{:S(2)}) collective-permute-start(bf16[4,192,128]{2,1,0:T(8,128)(2,1)S(1)} %copy-done.4), channel_id=1, source_target_pairs={{0,10},{2,8},{4,14},{6,12},{8,2},{10,0},{12,6},{14,4},{1,11},{3,9}... | collective-permute-start | bytes 589832 | tf_op jit(solution)/shard_map/ppermute | solution.py:195
  150.5 0.9 place.13.refs_0_
  151.4 2.9 %collective-permute-done.4.block_ref = bf16[4,832,128]{2,1,0:T(8,128)(2,1)S(1)} collective-permute-done((bf16[4,832,128]{2,1,0:T(8,128)(2,1)}, bf16[4,832,128]{2,1,0:T(8,128)(2,1)S(1)}, u32[]{:S(2)}, u32[]{:S(2)}) %collective-permute-start.4) | collective-permute-done | bytes 852000 | tf_op jit(solution)/shard_map/ppermute | solution.py:195
  155.2 2.0 %place.15.refs_0_ = bf16[4,6144,128]{2,1,0:T(8,128)(2,1)} custom-call(bf16[4,704,128]{2,1,0:T(8,128)(2,1)} %collective-permute-done.2.block_ref, bf16[4,6144,128]{2,1,0:T(8,128)(2,1)} %place.14.refs_0_), custom_call_target="tpu_custom_call", output_to_operand_aliasing={{}: (1, {})} | custom-call | flops 360448 | bytes 1441792 | tf_op jit(solution)/shard_map/place/pallas_call | solution.py:88
  157.2 13.9 %collective-permute-done.1.block_ref = bf16[4,512,128]{2,1,0:T(8,128)(2,1)S(1)} collective-permute-done((bf16[4,512,128]{2,1,0:T(8,128)(2,1)}, bf16[4,512,128]{2,1,0:T(8,128)(2,1)S(1)}, u32[]{:S(2)}, u32[]{:S(2)}) %collective-permute-start.1) | collective-permute-done | bytes 524320 | tf_op jit(solution)/shard_map/ppermute | solution.py:195
  171.9 3.3 %collective-permute-done.block_ref = bf16[4,192,128]{2,1,0:T(8,128)(2,1)S(1)} collective-permute-done((bf16[4,192,128]{2,1,0:T(8,128)(2,1)S(1)}, bf16[4,192,128]{2,1,0:T(8,128)(2,1)S(1)}, u32[]{:S(2)}, u32[]{:S(2)}) %collective-permute-start) | collective-permute-done | bytes 196640 | tf_op jit(solution)/shard_map/ppermute | solution.py:195
  (56 shorter events, 12.9 us)
Async XLA Ops:
  1.8 18.1 %copy-start.3 = (f32[8,4,768]{2,1,0:T(4,128)}, f32[8,4,768]{2,1,0:T(4,128)S(1)}, u32[]{:S(2)}) copy-start(f32[8,4,768]{2,1,0:T(4,128)S(1)} %reshape_reshape_squeeze.5.gates_ref) | copy-start | bytes 294916
  3.8 39.7 %all-to-all-start = ((bf16[8,4,850]{2,1,0:T(4,128)(2,1)}), bf16[8,4,850]{2,1,0:T(4,128)(2,1)S(1)}, u32[]{:S(2)}, u32[]{:S(2)}) async-start(bf16[8,4,850]{2,1,0:T(4,128)(2,1)} %concatenate.7), calls=%async_computation | async-start | bytes 114688 | tf_op jit(solution)/shard_map/all_to_all | solution.py:198
  12.1 62.5 %collective-permute-start.3 = (bf16[64,2048]{1,0:T(8,128)(2,1)S(1)}, bf16[64,2048]{1,0:T(8,128)(2,1)S(1)}, u32[]{:S(2)}, u32[]{:S(2)}) collective-permute-start(bf16[64,2048]{1,0:T(8,128)(2,1)S(1)} %slice_bitcast_fusion), channel_id=1, source_target_pairs={{0,8},{2,10},{4,12},{6,14},{8,0},{10,2},{12,4},{14,6},{1,9},{3,11}... | collective-permute-start | bytes 786440 | tf_op jit(solution)/shard_map/ppermute | solution.py:195
  15.1 85.5 %collective-permute-start.9 = (f32[4,4,64]{2,1,0:T(4,128)S(1)}, f32[4,4,64]{2,1,0:T(4,128)S(1)}, u32[]{:S(2)}, u32[]{:S(2)}) collective-permute-start(f32[4,4,64]{2,1,0:T(4,128)S(1)} %constant_dynamic-slice_fusion), channel_id=1, source_target_pairs={{0,8},{2,10},{4,12},{6,14},{8,0},{10,2},{12,4},{14,6},{1,9},{3,11}... | collective-permute-start | bytes 12296 | tf_op jit(solution)/shard_map/ppermute | solution.py:195
  19.9 97.8 %collective-permute-start.8 = (bf16[4,704,128]{2,1,0:T(8,128)(2,1)}, bf16[4,704,128]{2,1,0:T(8,128)(2,1)S(1)}, u32[]{:S(2)}, u32[]{:S(2)}) collective-permute-start(bf16[4,704,128]{2,1,0:T(8,128)(2,1)} %project.14.refs_1_), channel_id=1, source_target_pairs={{0,14},{2,12},{4,10},{6,8},{8,6},{10,4},{12,2},{14,0},{1,15},{3,13... | collective-permute-start | bytes 2162696 | tf_op jit(solution)/shard_map/ppermute | solution.py:195
  29.3 110.9 %collective-permute-start.7 = (bf16[4,704,128]{2,1,0:T(8,128)(2,1)}, bf16[4,704,128]{2,1,0:T(8,128)(2,1)}, u32[]{:S(2)}, u32[]{:S(2)}) collective-permute-start(bf16[4,704,128]{2,1,0:T(8,128)(2,1)} %project.13.refs_2_), channel_id=1, source_target_pairs={{0,12},{2,14},{4,8},{6,10},{8,4},{10,6},{12,0},{14,2},{1,13},{3,15... | collective-permute-start | bytes 2162696 | tf_op jit(solution)/shard_map/ppermute | solution.py:195
  34.7 120.6 %collective-permute-start.2 = (bf16[4,704,128]{2,1,0:T(8,128)(2,1)}, bf16[4,704,128]{2,1,0:T(8,128)(2,1)}, u32[]{:S(2)}, u32[]{:S(2)}) collective-permute-start(bf16[4,704,128]{2,1,0:T(8,128)(2,1)} %project.9.refs_6_), channel_id=1, source_target_pairs={{0,8},{2,10},{4,12},{6,14},{8,0},{10,2},{12,4},{14,6},{1,9},{3,11}... | collective-permute-start | bytes 2162696 | tf_op jit(solution)/shard_map/ppermute | solution.py:195
  83.7 61.5 %collective-permute-start.6 = (bf16[4,832,128]{2,1,0:T(8,128)(2,1)}, bf16[4,832,128]{2,1,0:T(8,128)(2,1)S(1)}, u32[]{:S(2)}, u32[]{:S(2)}) collective-permute-start(bf16[4,832,128]{2,1,0:T(8,128)(2,1)} %project.12.refs_3_), channel_id=1, source_target_pairs={{0,2},{2,0},{4,6},{6,4},{8,10},{10,8},{12,14},{14,12},{1,3},{3,1},... | collective-permute-start | bytes 2555912 | tf_op jit(solution)/shard_map/ppermute | solution.py:195
  100.6 22.5 %copy-start = (bf16[4,832,128]{2,1,0:T(8,128)(2,1)S(1)}, bf16[4,832,128]{2,1,0:T(8,128)(2,1)}, u32[]{:S(2)}) copy-start(bf16[4,832,128]{2,1,0:T(8,128)(2,1)} %project.15.block_ref.refs_0_) | copy-start | bytes 2555908
  100.6 0.6 copy-start.5
  100.6 49.9 %collective-permute-start.5 = (bf16[4,832,128]{2,1,0:T(8,128)(2,1)}, bf16[4,832,128]{2,1,0:T(8,128)(2,1)S(1)}, u32[]{:S(2)}, u32[]{:S(2)}) collective-permute-start(bf16[4,832,128]{2,1,0:T(8,128)(2,1)} %project.11.refs_4_), channel_id=1, source_target_pairs={{0,4},{2,6},{4,0},{6,2},{8,12},{10,14},{12,8},{14,10},{1,5},{3,7},... | collective-permute-start | bytes 2555912 | tf_op jit(solution)/shard_map/ppermute | solution.py:195
  114.3 24.1 %all-to-all-start.1 = ((f32[8,4,128]{2,1,0:T(4,128)}), f32[8,4,128]{2,1,0:T(4,128)S(1)}, u32[]{:S(2)}, u32[]{:S(2)}) async-start(f32[8,4,128]{2,1,0:T(4,128)} %read.1), calls=%async_computation.1 | async-start | bytes 32768 | tf_op jit(solution)/shard_map/all_to_all | solution.py:198
  117.7 0.9 copy-start.1
  118.5 35.8 %collective-permute-start.4 = (bf16[4,832,128]{2,1,0:T(8,128)(2,1)}, bf16[4,832,128]{2,1,0:T(8,128)(2,1)S(1)}, u32[]{:S(2)}, u32[]{:S(2)}) collective-permute-start(bf16[4,832,128]{2,1,0:T(8,128)(2,1)} %project.10.refs_5_), channel_id=1, source_target_pairs={{0,6},{2,4},{4,2},{6,0},{8,14},{10,12},{12,10},{14,8},{1,7},{3,5},... | collective-permute-start | bytes 2555912 | tf_op jit(solution)/shard_map/ppermute | solution.py:195
  140.2 30.9 %collective-permute-start.1 = (bf16[4,512,128]{2,1,0:T(8,128)(2,1)}, bf16[4,512,128]{2,1,0:T(8,128)(2,1)S(1)}, u32[]{:S(2)}, u32[]{:S(2)}) collective-permute-start(bf16[4,512,128]{2,1,0:T(8,128)(2,1)} %slice.49), channel_id=1, source_target_pairs={{0,10},{2,8},{4,14},{6,12},{8,2},{10,0},{12,6},{14,4},{1,11},{3,9}... | collective-permute-start | bytes 1572872 | tf_op jit(solution)/shard_map/ppermute | solution.py:195
  141.1 1.1 copy-start.2
  143.2 2.0 %copy-start.4 = (bf16[4,192,128]{2,1,0:T(8,128)(2,1)S(1)}, bf16[4,192,128]{2,1,0:T(8,128)(2,1)}, u32[]{:S(2)}) copy-start(bf16[4,192,128]{2,1,0:T(8,128)(2,1)} %slice.48) | copy-start | bytes 589828
  145.2 30.0 %collective-permute-start = (bf16[4,192,128]{2,1,0:T(8,128)(2,1)S(1)}, bf16[4,192,128]{2,1,0:T(8,128)(2,1)S(1)}, u32[]{:S(2)}, u32[]{:S(2)}) collective-permute-start(bf16[4,192,128]{2,1,0:T(8,128)(2,1)S(1)} %copy-done.4), channel_id=1, source_target_pairs={{0,10},{2,8},{4,14},{6,12},{8,2},{10,0},{12,6},{14,4},{1,11},{3,9}... | collective-permute-start | bytes 589832 | tf_op jit(solution)/shard_map/ppermute | solution.py:195
where the time goes:
time: 177 us; the launch traced here: 176 us
  waiting for transfers between devices  63.9 us (36%)
  Pallas kernels  62.6 us (35%)
  starting transfers between devices  27.9 us (16%)
  local copies, waits for them, and re-layouts  10.3 us (6%)
  other arithmetic  8.57 us (5%)
  blocking collectives  1.82 us (1%)
    ppermute x10, waiting for transfers between devices, swap(): return lax.ppermute(value, 'sp', [(i, i ^ step) for i in range(places)])  49.4 us
    pallas_call x8, Pallas kernels, project(): pl.pallas_call(functools.partial(project_block, step), grid_spec=pltpu.Pr...  39.5 us
    ppermute x10, starting transfers between devices, swap(): return lax.ppermute(value, 'sp', [(i, i ^ step) for i in range(places)])  17.2 us
    all_to_all x2, waiting for transfers between devices, exchange(): return lax.all_to_all(value, 'sp', split_axis=0, concat_axis=0, tiled=True)  14.4 us
    pallas_call x1, Pallas kernels, partial_reads(): pl.pallas_call(functools.partial(read_blocks, steps, near), in_specs=[pl....  13.1 us
    all_to_all x2, starting transfers between devices, exchange(): return lax.all_to_all(value, 'sp', split_axis=0, concat_axis=0, tiled=True)  10.7 us
    pallas_call x9, Pallas kernels, place(): pl.pallas_call(functools.partial(place_block, parts, length), in_specs=[p...  9.98 us
    concatenate x1, other arithmetic, on_device(): more = jnp.concatenate([rows, lent], axis=0)  4.09 us
  transfers between devices with their start and end apart: 12, of which 5 were waited for; matrix products, arithmetic and copies ran while one was open for 8% of the time, Pallas kernels for 35%

commit v1 on v0

--- a/solution.py
+++ b/solution.py
@@ -175,9 +175,10 @@
 
 def plan(places):
     far = places // 2
-    across, near = list(range(far, places)), list(range(1, far))
+    across = [places - 1] + list(range(far, places - 1))
+    near = [far // 2] + [step for step in range(1, far) if step != far // 2]
     half = len(across) // 2
-    order = across[half:][::-1] + near + across[:half]
+    order = across[:half] + near + across[half:]
     return order[:-1], order[-1:]
 
 

time: 177 us -> 175 us (0.989)
  waiting for transfers between devices: 63.9 us -> 60.2 us
  starting transfers between devices: 27.9 us -> 30.2 us
    ppermute x10, waiting for transfers between devices: 49.4 us -> 46.3 us  [swap(): return lax.ppermute(value, 'sp', [(i, i ^ step) for i in range(places)])]
    ppermute x10, starting transfers between devices: 17.2 us -> 19 us  [swap(): return lax.ppermute(value, 'sp', [(i, i ^ step) for i in range(places)])]
  transfers between devices with their start and end apart: 12 -> 12, of which waited for: 5 -> 3; matrix products, arithmetic and copies ran while one was open for 8% -> 8% of each run, Pallas kernels for 35% -> 36%
where the time goes in v1:
time: 175 us; the launch traced here: 174 us
  Pallas kernels  62.7 us (36%)
  waiting for transfers between devices  60.2 us (34%)
  starting transfers between devices  30.2 us (17%)
  local copies, waits for them, and re-layouts  9.77 us (6%)
  other arithmetic  8.57 us (5%)
  blocking collectives  1.82 us (1%)
    ppermute x10, waiting for transfers between devices, swap(): return lax.ppermute(value, 'sp', [(i, i ^ step) for i in range(places)])  46.3 us
    pallas_call x8, Pallas kernels, project(): pl.pallas_call(functools.partial(project_block, step), grid_spec=pltpu.Pr...  39.5 us
    ppermute x10, starting transfers between devices, swap(): return lax.ppermute(value, 'sp', [(i, i ^ step) for i in range(places)])  19 us
    all_to_all x2, waiting for transfers between devices, exchange(): return lax.all_to_all(value, 'sp', split_axis=0, concat_axis=0, tiled=True)  13.8 us
    pallas_call x1, Pallas kernels, partial_reads(): pl.pallas_call(functools.partial(read_blocks, steps, near), in_specs=[pl....  13.1 us
    all_to_all x2, starting transfers between devices, exchange(): return lax.all_to_all(value, 'sp', split_axis=0, concat_axis=0, tiled=True)  11.2 us
    pallas_call x9, Pallas kernels, place(): pl.pallas_call(functools.partial(place_block, parts, length), in_specs=[p...  10 us
    concatenate x1, other arithmetic, on_device(): more = jnp.concatenate([rows, lent], axis=0)  4.09 us
  transfers between devices with their start and end apart: 12, of which 3 were waited for; matrix products, arithmetic and copies ran while one was open for 8% of the time, Pallas kernels for 36%

profile of v1, /device:TPU:0, one launch (start us, length us, event | category | flops | bytes accessed | tf_op | source)
XLA Modules:
  0.0 174.1 jit_solution(4327134096834853186)
XLA Ops:
  0.6 1.1 reduce.2
  3.8 7.3 %all-to-all-start = ((bf16[8,4,850]{2,1,0:T(4,128)(2,1)}), bf16[8,4,850]{2,1,0:T(4,128)(2,1)S(1)}, u32[]{:S(2)}, u32[]{:S(2)}) async-start(bf16[8,4,850]{2,1,0:T(4,128)(2,1)} %concatenate.7), calls=%async_computation | async-start | bytes 114688 | tf_op jit(solution)/shard_map/all_to_all | solution.py:199
  11.1 1.0 slice_bitcast_fusion
  12.1 3.0 %collective-permute-start.3 = (bf16[64,2048]{1,0:T(8,128)(2,1)S(1)}, bf16[64,2048]{1,0:T(8,128)(2,1)S(1)}, u32[]{:S(2)}, u32[]{:S(2)}) collective-permute-start(bf16[64,2048]{1,0:T(8,128)(2,1)S(1)} %slice_bitcast_fusion), channel_id=1, source_target_pairs={{0,8},{2,10},{4,12},{6,14},{8,0},{10,2},{12,4},{14,6},{1,9},{3,11}... | collective-permute-start | bytes 786440 | tf_op jit(solution)/shard_map/ppermute | solution.py:196
  15.2 4.7 %project.14.refs_1_ = bf16[4,704,128]{2,1,0:T(8,128)(2,1)} custom-call(s32[1]{0:T(128)} %bitcast.me_ref, bf16[768,2048]{1,0:T(8,128)(2,1)} %bitcast.26, bf16[2048,2048]{1,0:T(8,128)(2,1)} %key_ref.15, bf16[2048,2048]{1,0:T(8,128)(2,1)} %value_ref.15), custom_call_target="tpu_custom_call" | custom-call | flops 1476395008 | bytes 5701632 | tf_op jit(solution)/shard_map/project/pallas_call | solution.py:48
  19.9 4.7 %collective-permute-start.8 = (bf16[4,704,128]{2,1,0:T(8,128)(2,1)}, bf16[4,704,128]{2,1,0:T(8,128)(2,1)S(1)}, u32[]{:S(2)}, u32[]{:S(2)}) collective-permute-start(bf16[4,704,128]{2,1,0:T(8,128)(2,1)} %project.14.refs_1_), channel_id=1, source_target_pairs={{0,14},{2,12},{4,10},{6,8},{8,6},{10,4},{12,2},{14,0},{1,15},{3,13... | collective-permute-start | bytes 2162696 | tf_op jit(solution)/shard_map/ppermute | solution.py:196
  24.6 4.7 %project.13.refs_2_ = bf16[4,704,128]{2,1,0:T(8,128)(2,1)} custom-call(s32[1]{0:T(128)} %bitcast.me_ref, bf16[768,2048]{1,0:T(8,128)(2,1)} %bitcast.27, bf16[2048,2048]{1,0:T(8,128)(2,1)} %key_ref.15, bf16[2048,2048]{1,0:T(8,128)(2,1)} %value_ref.15), custom_call_target="tpu_custom_call" | custom-call | flops 1476395008 | bytes 5701632 | tf_op jit(solution)/shard_map/project/pallas_call | solution.py:48
  29.3 4.8 %project.9.refs_6_ = bf16[4,704,128]{2,1,0:T(8,128)(2,1)} custom-call(s32[1]{0:T(128)} %bitcast.me_ref, bf16[768,2048]{1,0:T(8,128)(2,1)} %bitcast.28, bf16[2048,2048]{1,0:T(8,128)(2,1)} %key_ref.15, bf16[2048,2048]{1,0:T(8,128)(2,1)} %value_ref.15), custom_call_target="tpu_custom_call" | custom-call | flops 1476395008 | bytes 5701632 | tf_op jit(solution)/shard_map/project/pallas_call | solution.py:48
  34.1 2.9 %collective-permute-start.2 = (bf16[4,704,128]{2,1,0:T(8,128)(2,1)}, bf16[4,704,128]{2,1,0:T(8,128)(2,1)}, u32[]{:S(2)}, u32[]{:S(2)}) collective-permute-start(bf16[4,704,128]{2,1,0:T(8,128)(2,1)} %project.9.refs_6_), channel_id=1, source_target_pairs={{0,10},{2,8},{4,14},{6,12},{8,2},{10,0},{12,6},{14,4},{1,11},{3,9}... | collective-permute-start | bytes 2162696 | tf_op jit(solution)/shard_map/ppermute | solution.py:196
  37.0 4.8 %project.8.refs_7_ = bf16[4,704,128]{2,1,0:T(8,128)(2,1)} custom-call(s32[1]{0:T(128)} %bitcast.me_ref, bf16[768,2048]{1,0:T(8,128)(2,1)} %bitcast.29, bf16[2048,2048]{1,0:T(8,128)(2,1)} %key_ref.15, bf16[2048,2048]{1,0:T(8,128)(2,1)} %value_ref.15), custom_call_target="tpu_custom_call" | custom-call | flops 1476395008 | bytes 5701632 | tf_op jit(solution)/shard_map/project/pallas_call | solution.py:48
  41.8 1.9 %slice.49 = bf16[4,512,128]{2,1,0:T(8,128)(2,1)} slice(bf16[4,704,128]{2,1,0:T(8,128)(2,1)} %project.8.refs_7_), slice={[0:4], [0:512], [0:128]} | slice | bytes 1048576 | tf_op jit(solution)/shard_map/slice | solution.py:220
  43.7 1.6 slice.48
  47.0 27.5 %collective-permute-done.3 = bf16[64,2048]{1,0:T(8,128)(2,1)S(1)} collective-permute-done((bf16[64,2048]{1,0:T(8,128)(2,1)S(1)}, bf16[64,2048]{1,0:T(8,128)(2,1)S(1)}, u32[]{:S(2)}, u32[]{:S(2)}) %collective-permute-start.3) | collective-permute-done | bytes 262176 | tf_op jit(solution)/shard_map/ppermute | solution.py:196
  74.5 4.1 %pad_maximum_fusion.tokens_ref = bf16[832,2048]{1,0:T(8,128)(2,1)} fusion(bf16[64,2048]{1,0:T(8,128)(2,1)S(1)} %collective-permute-done.3, bf16[768,2048]{1,0:T(8,128)(2,1)} %bitcast.30), kind=kLoop, calls=%fused_computation | loop fusion | flops 6815744 | bytes 6815744 | tf_op jit(solution)/shard_map/concatenate | solution.py:202
  78.6 5.1 %project.12.refs_3_ = bf16[4,832,128]{2,1,0:T(8,128)(2,1)} custom-call(s32[1]{0:T(128)} %bitcast.me_ref, bf16[832,2048]{1,0:T(8,128)(2,1)} %pad_maximum_fusion.tokens_ref, bf16[2048,2048]{1,0:T(8,128)(2,1)} %key_ref.15, bf16[2048,2048]{1,0:T(8,128)(2,1)} %value_ref.15), custom_call_target="tpu_custom_call" | custom-call | flops 1744830464 | bytes 6356992 | tf_op jit(solution)/shard_map/project/pallas_call | solution.py:48
  83.7 5.1 %project.10.refs_5_ = bf16[4,832,128]{2,1,0:T(8,128)(2,1)} custom-call(s32[1]{0:T(128)} %bitcast.me_ref, bf16[832,2048]{1,0:T(8,128)(2,1)} %pad_maximum_fusion.tokens_ref, bf16[2048,2048]{1,0:T(8,128)(2,1)} %key_ref.15, bf16[2048,2048]{1,0:T(8,128)(2,1)} %value_ref.15), custom_call_target="tpu_custom_call" | custom-call | flops 1744830464 | bytes 6356992 | tf_op jit(solution)/shard_map/project/pallas_call | solution.py:48
  88.8 5.1 %project.11.refs_4_ = bf16[4,832,128]{2,1,0:T(8,128)(2,1)} custom-call(s32[1]{0:T(128)} %bitcast.me_ref, bf16[832,2048]{1,0:T(8,128)(2,1)} %pad_maximum_fusion.tokens_ref, bf16[2048,2048]{1,0:T(8,128)(2,1)} %key_ref.15, bf16[2048,2048]{1,0:T(8,128)(2,1)} %value_ref.15), custom_call_target="tpu_custom_call" | custom-call | flops 1744830464 | bytes 6356992 | tf_op jit(solution)/shard_map/project/pallas_call | solution.py:48
  94.0 5.2 %project.15.block_ref.refs_0_ = bf16[4,832,128]{2,1,0:T(8,128)(2,1)} custom-call(s32[1]{0:T(128)} %bitcast.me_ref, bf16[832,2048]{1,0:T(8,128)(2,1)} %pad_maximum_fusion.tokens_ref, bf16[2048,2048]{1,0:T(8,128)(2,1)} %key_ref.15, bf16[2048,2048]{1,0:T(8,128)(2,1)} %value_ref.15), custom_call_target="tpu_custom_call" | custom-call | flops 1744830464 | bytes 6356992 | tf_op jit(solution)/shard_map/project/pallas_call | solution.py:48
  99.2 1.5 collective-permute-start.5
  100.7 13.1 %read.1 = f32[8,4,128]{2,1,0:T(4,128)} custom-call(s32[1]{0:T(128)} %bitcast.me_ref, f32[8,4,128]{2,1,0:T(4,128)} %pad_convert_fusion.query_ref, f32[8,4,768]{2,1,0:T(4,128)} %copy-done.3, f32[4,4,64]{2,1,0:T(4,128)} %copy-done.5, bf16[4,832,128]{2,1,0:T(8,128)(2,1)} %project.15.block_ref.refs_0_, bf16[4,704,128]{2,1,0:T(8,128)(2,1)} %project.14.refs_1_, ...), custom_call_target="tpu_custom_call" | custom-call | flops 50331648 | bytes 6291456 | tf_op jit(solution)/shard_map/read/pallas_call | solution.py:132
  113.8 3.9 %all-to-all-start.1 = ((f32[8,4,128]{2,1,0:T(4,128)}), f32[8,4,128]{2,1,0:T(4,128)S(1)}, u32[]{:S(2)}, u32[]{:S(2)}) async-start(f32[8,4,128]{2,1,0:T(4,128)} %read.1), calls=%async_computation.1 | async-start | bytes 32768 | tf_op jit(solution)/shard_map/all_to_all | solution.py:199
  118.5 2.9 %collective-permute-start.4 = (bf16[4,832,128]{2,1,0:T(8,128)(2,1)}, bf16[4,832,128]{2,1,0:T(8,128)(2,1)S(1)}, u32[]{:S(2)}, u32[]{:S(2)}) collective-permute-start(bf16[4,832,128]{2,1,0:T(8,128)(2,1)} %project.10.refs_5_), channel_id=1, source_target_pairs={{0,6},{2,4},{4,2},{6,0},{8,14},{10,12},{12,10},{14,8},{1,7},{3,5},... | collective-permute-start | bytes 2555912 | tf_op jit(solution)/shard_map/ppermute | solution.py:196
  121.5 1.6 slice_add_fusion
  124.0 13.8 %all-to-all-done.1 = f32[8,4,128]{2,1,0:T(4,128)S(1)} async-done(((f32[8,4,128]{2,1,0:T(4,128)}), f32[8,4,128]{2,1,0:T(4,128)S(1)}, u32[]{:S(2)}, u32[]{:S(2)}) %all-to-all-start.1) | async-done | bytes 16416 | tf_op jit(solution)/shard_map/all_to_all | solution.py:199
  137.8 1.8 %all_gather.3 = f32[16,4,128]{2,1,0:T(4,128)S(1)} all-gather(f32[8,4,128]{2,1,0:T(4,128)S(1)} %all-to-all-done.1), channel_id=1, replica_groups=mesh['gr'=2,'sp'=8,'tp'=2] {'tp'}, dimensions={0}, use_global_device_ids=true | all-gather | bytes 49152 | tf_op jit(solution)/shard_map/all_gather | solution.py:239
  139.6 2.1 %collective-permute-start.1 = (bf16[4,512,128]{2,1,0:T(8,128)(2,1)}, bf16[4,512,128]{2,1,0:T(8,128)(2,1)S(1)}, u32[]{:S(2)}, u32[]{:S(2)}) collective-permute-start(bf16[4,512,128]{2,1,0:T(8,128)(2,1)} %slice.49), channel_id=1, source_target_pairs={{0,12},{2,14},{4,8},{6,10},{8,4},{10,6},{12,0},{14,2},{1,13},{3,15... | collective-permute-start | bytes 1572872 | tf_op jit(solution)/shard_map/ppermute | solution.py:196
  142.4 1.1 copy-done.2
  144.5 2.0 %place.11.refs_0_ = bf16[4,6144,128]{2,1,0:T(8,128)(2,1)} custom-call(bf16[4,704,128]{2,1,0:T(8,128)(2,1)} %collective-permute-done.7.block_ref, bf16[4,6144,128]{2,1,0:T(8,128)(2,1)} %place.10.refs_0_), custom_call_target="tpu_custom_call", output_to_operand_aliasing={{}: (1, {})} | custom-call | flops 360448 | bytes 1441792 | tf_op jit(solution)/shard_map/place/pallas_call | solution.py:88
  146.5 1.8 %collective-permute-start = (bf16[4,192,128]{2,1,0:T(8,128)(2,1)S(1)}, bf16[4,192,128]{2,1,0:T(8,128)(2,1)S(1)}, u32[]{:S(2)}, u32[]{:S(2)}) collective-permute-start(bf16[4,192,128]{2,1,0:T(8,128)(2,1)S(1)} %copy-done.4), channel_id=1, source_target_pairs={{0,12},{2,14},{4,8},{6,10},{8,4},{10,6},{12,0},{14,2},{1,13},{3,15... | collective-permute-start | bytes 589832 | tf_op jit(solution)/shard_map/ppermute | solution.py:196
  149.9 0.9 place.13.refs_0_
  150.8 18.8 %collective-permute-done.4.block_ref = bf16[4,832,128]{2,1,0:T(8,128)(2,1)S(1)} collective-permute-done((bf16[4,832,128]{2,1,0:T(8,128)(2,1)}, bf16[4,832,128]{2,1,0:T(8,128)(2,1)S(1)}, u32[]{:S(2)}, u32[]{:S(2)}) %collective-permute-start.4) | collective-permute-done | bytes 852000 | tf_op jit(solution)/shard_map/ppermute | solution.py:196
  170.5 2.0 %place.15.refs_0_ = bf16[4,6144,128]{2,1,0:T(8,128)(2,1)} custom-call(bf16[4,704,128]{2,1,0:T(8,128)(2,1)} %collective-permute-done.2.block_ref, bf16[4,6144,128]{2,1,0:T(8,128)(2,1)} %place.14.refs_0_), custom_call_target="tpu_custom_call", output_to_operand_aliasing={{}: (1, {})} | custom-call | flops 360448 | bytes 1441792 | tf_op jit(solution)/shard_map/place/pallas_call | solution.py:88
  (56 shorter events, 11.1 us)
Async XLA Ops:
  1.8 18.1 %copy-start.3 = (f32[8,4,768]{2,1,0:T(4,128)}, f32[8,4,768]{2,1,0:T(4,128)S(1)}, u32[]{:S(2)}) copy-start(f32[8,4,768]{2,1,0:T(4,128)S(1)} %reshape_reshape_squeeze.5.gates_ref) | copy-start | bytes 294916
  3.8 41.5 %all-to-all-start = ((bf16[8,4,850]{2,1,0:T(4,128)(2,1)}), bf16[8,4,850]{2,1,0:T(4,128)(2,1)S(1)}, u32[]{:S(2)}, u32[]{:S(2)}) async-start(bf16[8,4,850]{2,1,0:T(4,128)(2,1)} %concatenate.7), calls=%async_computation | async-start | bytes 114688 | tf_op jit(solution)/shard_map/all_to_all | solution.py:199
  12.1 62.5 %collective-permute-start.3 = (bf16[64,2048]{1,0:T(8,128)(2,1)S(1)}, bf16[64,2048]{1,0:T(8,128)(2,1)S(1)}, u32[]{:S(2)}, u32[]{:S(2)}) collective-permute-start(bf16[64,2048]{1,0:T(8,128)(2,1)S(1)} %slice_bitcast_fusion), channel_id=1, source_target_pairs={{0,8},{2,10},{4,12},{6,14},{8,0},{10,2},{12,4},{14,6},{1,9},{3,11}... | collective-permute-start | bytes 786440 | tf_op jit(solution)/shard_map/ppermute | solution.py:196
  15.1 84.0 %collective-permute-start.9 = (f32[4,4,64]{2,1,0:T(4,128)S(1)}, f32[4,4,64]{2,1,0:T(4,128)S(1)}, u32[]{:S(2)}, u32[]{:S(2)}) collective-permute-start(f32[4,4,64]{2,1,0:T(4,128)S(1)} %constant_dynamic-slice_fusion), channel_id=1, source_target_pairs={{0,8},{2,10},{4,12},{6,14},{8,0},{10,2},{12,4},{14,6},{1,9},{3,11}... | collective-permute-start | bytes 12296 | tf_op jit(solution)/shard_map/ppermute | solution.py:196
  19.9 97.8 %collective-permute-start.8 = (bf16[4,704,128]{2,1,0:T(8,128)(2,1)}, bf16[4,704,128]{2,1,0:T(8,128)(2,1)S(1)}, u32[]{:S(2)}, u32[]{:S(2)}) collective-permute-start(bf16[4,704,128]{2,1,0:T(8,128)(2,1)} %project.14.refs_1_), channel_id=1, source_target_pairs={{0,14},{2,12},{4,10},{6,8},{8,6},{10,4},{12,2},{14,0},{1,15},{3,13... | collective-permute-start | bytes 2162696 | tf_op jit(solution)/shard_map/ppermute | solution.py:196
  29.3 110.3 %collective-permute-start.7 = (bf16[4,704,128]{2,1,0:T(8,128)(2,1)}, bf16[4,704,128]{2,1,0:T(8,128)(2,1)}, u32[]{:S(2)}, u32[]{:S(2)}) collective-permute-start(bf16[4,704,128]{2,1,0:T(8,128)(2,1)} %project.13.refs_2_), channel_id=1, source_target_pairs={{0,8},{2,10},{4,12},{6,14},{8,0},{10,2},{12,4},{14,6},{1,9},{3,11}... | collective-permute-start | bytes 2162696 | tf_op jit(solution)/shard_map/ppermute | solution.py:196
  34.1 136.4 %collective-permute-start.2 = (bf16[4,704,128]{2,1,0:T(8,128)(2,1)}, bf16[4,704,128]{2,1,0:T(8,128)(2,1)}, u32[]{:S(2)}, u32[]{:S(2)}) collective-permute-start(bf16[4,704,128]{2,1,0:T(8,128)(2,1)} %project.9.refs_6_), channel_id=1, source_target_pairs={{0,10},{2,8},{4,14},{6,12},{8,2},{10,0},{12,6},{14,4},{1,11},{3,9}... | collective-permute-start | bytes 2162696 | tf_op jit(solution)/shard_map/ppermute | solution.py:196
  83.7 62.8 %collective-permute-start.6 = (bf16[4,832,128]{2,1,0:T(8,128)(2,1)}, bf16[4,832,128]{2,1,0:T(8,128)(2,1)S(1)}, u32[]{:S(2)}, u32[]{:S(2)}) collective-permute-start(bf16[4,832,128]{2,1,0:T(8,128)(2,1)} %project.12.refs_3_), channel_id=1, source_target_pairs={{0,4},{2,6},{4,0},{6,2},{8,12},{10,14},{12,8},{14,10},{1,5},{3,7},... | collective-permute-start | bytes 2555912 | tf_op jit(solution)/shard_map/ppermute | solution.py:196
  99.1 23.9 %copy-start = (bf16[4,832,128]{2,1,0:T(8,128)(2,1)S(1)}, bf16[4,832,128]{2,1,0:T(8,128)(2,1)}, u32[]{:S(2)}) copy-start(bf16[4,832,128]{2,1,0:T(8,128)(2,1)} %project.15.block_ref.refs_0_) | copy-start | bytes 2555908
  99.1 1.5 copy-start.5
  99.2 50.7 %collective-permute-start.5 = (bf16[4,832,128]{2,1,0:T(8,128)(2,1)}, bf16[4,832,128]{2,1,0:T(8,128)(2,1)S(1)}, u32[]{:S(2)}, u32[]{:S(2)}) collective-permute-start(bf16[4,832,128]{2,1,0:T(8,128)(2,1)} %project.11.refs_4_), channel_id=1, source_target_pairs={{0,2},{2,0},{4,6},{6,4},{8,10},{10,8},{12,14},{14,12},{1,3},{3,1},... | collective-permute-start | bytes 2555912 | tf_op jit(solution)/shard_map/ppermute | solution.py:196
  113.8 24.0 %all-to-all-start.1 = ((f32[8,4,128]{2,1,0:T(4,128)}), f32[8,4,128]{2,1,0:T(4,128)S(1)}, u32[]{:S(2)}, u32[]{:S(2)}) async-start(f32[8,4,128]{2,1,0:T(4,128)} %read.1), calls=%async_computation.1 | async-start | bytes 32768 | tf_op jit(solution)/shard_map/all_to_all | solution.py:199
  117.7 0.9 copy-start.1
  118.5 51.1 %collective-permute-start.4 = (bf16[4,832,128]{2,1,0:T(8,128)(2,1)}, bf16[4,832,128]{2,1,0:T(8,128)(2,1)S(1)}, u32[]{:S(2)}, u32[]{:S(2)}) collective-permute-start(bf16[4,832,128]{2,1,0:T(8,128)(2,1)} %project.10.refs_5_), channel_id=1, source_target_pairs={{0,6},{2,4},{4,2},{6,0},{8,14},{10,12},{12,10},{14,8},{1,7},{3,5},... | collective-permute-start | bytes 2555912 | tf_op jit(solution)/shard_map/ppermute | solution.py:196
  139.6 32.9 %collective-permute-start.1 = (bf16[4,512,128]{2,1,0:T(8,128)(2,1)}, bf16[4,512,128]{2,1,0:T(8,128)(2,1)S(1)}, u32[]{:S(2)}, u32[]{:S(2)}) collective-permute-start(bf16[4,512,128]{2,1,0:T(8,128)(2,1)} %slice.49), channel_id=1, source_target_pairs={{0,12},{2,14},{4,8},{6,10},{8,4},{10,6},{12,0},{14,2},{1,13},{3,15... | collective-permute-start | bytes 1572872 | tf_op jit(solution)/shard_map/ppermute | solution.py:196
  142.4 1.1 copy-start.2
  144.5 2.0 %copy-start.4 = (bf16[4,192,128]{2,1,0:T(8,128)(2,1)S(1)}, bf16[4,192,128]{2,1,0:T(8,128)(2,1)}, u32[]{:S(2)}) copy-start(bf16[4,192,128]{2,1,0:T(8,128)(2,1)} %slice.48) | copy-start | bytes 589828
  146.5 26.9 %collective-permute-start = (bf16[4,192,128]{2,1,0:T(8,128)(2,1)S(1)}, bf16[4,192,128]{2,1,0:T(8,128)(2,1)S(1)}, u32[]{:S(2)}, u32[]{:S(2)}) collective-permute-start(bf16[4,192,128]{2,1,0:T(8,128)(2,1)S(1)} %copy-done.4), channel_id=1, source_target_pairs={{0,12},{2,14},{4,8},{6,10},{8,4},{10,6},{12,0},{14,2},{1,13},{3,15... | collective-permute-start | bytes 589832 | tf_op jit(solution)/shard_map/ppermute | solution.py:196

commit v2 on v1

--- a/solution.py
+++ b/solution.py
@@ -187,6 +187,7 @@
     rows = tokens[0, 0]
     length = rows.shape[0]
     far = places // 2
+    peer = far + far // 2
     me = lax.axis_index("sp").astype(jnp.int32)
     here = me.reshape(1)
     early, late = plan(places)
@@ -198,7 +199,7 @@
     def exchange(value):
         return lax.all_to_all(value, "sp", split_axis=0, concat_axis=0, tiled=True)
 
-    lent = swap(rows[kept:], far)
+    lent = swap(rows[kept:], peer)
     more = jnp.concatenate([rows, lent], axis=0)
 
     def block_of(step):
@@ -207,7 +208,7 @@
 
     def parts_of(step):
         if step < far:
-            return ((step, 0, 0, length), (step ^ far, kept, length, ROWS))
+            return ((step, 0, 0, length), (step ^ peer, kept, length, ROWS))
         return ((step, 0, 0, kept),)
 
     sent, arrived = {}, []
@@ -229,7 +230,7 @@
     queries = told[:, :, -size:]
     gate_parts = unpacked_gates(told[:, :, :-size], length)
     gate_cache = jnp.transpose(gate_parts, (1, 0, 2)).reshape(1, heads, places * length)
-    borrowed = swap(lax.dynamic_slice(gates, ((me ^ far) & far, 0, kept), (far, heads, ROWS)), far)
+    borrowed = swap(lax.dynamic_slice(gates, ((me ^ far) & far, 0, kept), (far, heads, ROWS)), peer)
 
     sent[0] = block_of(0)
     cache = place(None, sent[0], parts_of(0), places, length)

time: 175 us -> 177 us (1.011)
  starting transfers between devices: 30.2 us -> 58.4 us
  waiting for transfers between devices: 60.2 us -> 34.3 us
    ppermute x10, waiting for transfers between devices: 46.3 us -> 5.28 us  [swap(): return lax.ppermute(value, 'sp', [(i, i ^ step) for i in range(places)])]
    ppermute x10, starting transfers between devices: 19 us -> 47.1 us  [swap(): return lax.ppermute(value, 'sp', [(i, i ^ step) for i in range(places)])]
    all_to_all x2, waiting for transfers between devices: 13.8 us -> 29 us  [exchange(): return lax.all_to_all(value, 'sp', split_axis=0, concat_axis=0, tiled=True)]
  transfers between devices with their start and end apart: 12 -> 12, of which waited for: 3 -> 3; matrix products, arithmetic and copies ran while one was open for 8% -> 8% of each run, Pallas kernels for 36% -> 35%
where the time goes in v2:
time: 177 us; the launch traced here: 176 us
  Pallas kernels  62.6 us (35%)
  starting transfers between devices  58.4 us (33%)
  waiting for transfers between devices  34.3 us (19%)
  local copies, waits for them, and re-layouts  9.77 us (6%)
  other arithmetic  8.57 us (5%)
  blocking collectives  1.82 us (1%)
    ppermute x10, starting transfers between devices, swap(): return lax.ppermute(value, 'sp', [(i, i ^ step) for i in range(places)])  47.1 us
    pallas_call x8, Pallas kernels, project(): pl.pallas_call(functools.partial(project_block, step), grid_spec=pltpu.Pr...  39.5 us
    all_to_all x2, waiting for transfers between devices, exchange(): return lax.all_to_all(value, 'sp', split_axis=0, concat_axis=0, tiled=True)  29 us
    pallas_call x1, Pallas kernels, partial_reads(): pl.pallas_call(functools.partial(read_blocks, steps, near), in_specs=[pl....  13.1 us
    all_to_all x2, starting transfers between devices, exchange(): return lax.all_to_all(value, 'sp', split_axis=0, concat_axis=0, tiled=True)  11.3 us
    pallas_call x9, Pallas kernels, place(): pl.pallas_call(functools.partial(place_block, parts, length), in_specs=[p...  10 us
    ppermute x10, waiting for transfers between devices, swap(): return lax.ppermute(value, 'sp', [(i, i ^ step) for i in range(places)])  5.28 us
    concatenate x1, other arithmetic, on_device(): more = jnp.concatenate([rows, lent], axis=0)  4.09 us
  transfers between devices with their start and end apart: 12, of which 3 were waited for; matrix products, arithmetic and copies ran while one was open for 8% of the time, Pallas kernels for 35%

profile of v2, /device:TPU:0, one launch (start us, length us, event | category | flops | bytes accessed | tf_op | source)
XLA Modules:
  0.0 176.4 jit_solution(4494040610543496191)
XLA Ops:
  0.6 1.1 reduce.2
  3.8 7.3 %all-to-all-start = ((bf16[8,4,850]{2,1,0:T(4,128)(2,1)}), bf16[8,4,850]{2,1,0:T(4,128)(2,1)S(1)}, u32[]{:S(2)}, u32[]{:S(2)}) async-start(bf16[8,4,850]{2,1,0:T(4,128)(2,1)} %concatenate.7), calls=%async_computation | async-start | bytes 114688 | tf_op jit(solution)/shard_map/all_to_all | solution.py:200
  11.1 1.0 slice_bitcast_fusion
  12.1 3.9 %collective-permute-start.3 = (bf16[64,2048]{1,0:T(8,128)(2,1)S(1)}, bf16[64,2048]{1,0:T(8,128)(2,1)S(1)}, u32[]{:S(2)}, u32[]{:S(2)}) collective-permute-start(bf16[64,2048]{1,0:T(8,128)(2,1)S(1)} %slice_bitcast_fusion), channel_id=1, source_target_pairs={{0,12},{2,14},{4,8},{6,10},{8,4},{10,6},{12,0},{14,2},{1,13},{3,15... | collective-permute-start | bytes 786440 | tf_op jit(solution)/shard_map/ppermute | solution.py:197
  16.1 4.7 %project.14.refs_1_ = bf16[4,704,128]{2,1,0:T(8,128)(2,1)} custom-call(s32[1]{0:T(128)} %bitcast.me_ref, bf16[768,2048]{1,0:T(8,128)(2,1)} %bitcast.26, bf16[2048,2048]{1,0:T(8,128)(2,1)} %key_ref.15, bf16[2048,2048]{1,0:T(8,128)(2,1)} %value_ref.15), custom_call_target="tpu_custom_call" | custom-call | flops 1476395008 | bytes 5701632 | tf_op jit(solution)/shard_map/project/pallas_call | solution.py:48
  20.8 4.7 %collective-permute-start.8 = (bf16[4,704,128]{2,1,0:T(8,128)(2,1)}, bf16[4,704,128]{2,1,0:T(8,128)(2,1)S(1)}, u32[]{:S(2)}, u32[]{:S(2)}) collective-permute-start(bf16[4,704,128]{2,1,0:T(8,128)(2,1)} %project.14.refs_1_), channel_id=1, source_target_pairs={{0,14},{2,12},{4,10},{6,8},{8,6},{10,4},{12,2},{14,0},{1,15},{3,13... | collective-permute-start | bytes 2162696 | tf_op jit(solution)/shard_map/ppermute | solution.py:197
  25.5 4.7 %project.13.refs_2_ = bf16[4,704,128]{2,1,0:T(8,128)(2,1)} custom-call(s32[1]{0:T(128)} %bitcast.me_ref, bf16[768,2048]{1,0:T(8,128)(2,1)} %bitcast.27, bf16[2048,2048]{1,0:T(8,128)(2,1)} %key_ref.15, bf16[2048,2048]{1,0:T(8,128)(2,1)} %value_ref.15), custom_call_target="tpu_custom_call" | custom-call | flops 1476395008 | bytes 5701632 | tf_op jit(solution)/shard_map/project/pallas_call | solution.py:48
  30.2 4.8 %project.9.refs_6_ = bf16[4,704,128]{2,1,0:T(8,128)(2,1)} custom-call(s32[1]{0:T(128)} %bitcast.me_ref, bf16[768,2048]{1,0:T(8,128)(2,1)} %bitcast.28, bf16[2048,2048]{1,0:T(8,128)(2,1)} %key_ref.15, bf16[2048,2048]{1,0:T(8,128)(2,1)} %value_ref.15), custom_call_target="tpu_custom_call" | custom-call | flops 1476395008 | bytes 5701632 | tf_op jit(solution)/shard_map/project/pallas_call | solution.py:48
  35.0 2.9 %collective-permute-start.2 = (bf16[4,704,128]{2,1,0:T(8,128)(2,1)}, bf16[4,704,128]{2,1,0:T(8,128)(2,1)}, u32[]{:S(2)}, u32[]{:S(2)}) collective-permute-start(bf16[4,704,128]{2,1,0:T(8,128)(2,1)} %project.9.refs_6_), channel_id=1, source_target_pairs={{0,10},{2,8},{4,14},{6,12},{8,2},{10,0},{12,6},{14,4},{1,11},{3,9}... | collective-permute-start | bytes 2162696 | tf_op jit(solution)/shard_map/ppermute | solution.py:197
  37.9 4.8 %project.8.refs_7_ = bf16[4,704,128]{2,1,0:T(8,128)(2,1)} custom-call(s32[1]{0:T(128)} %bitcast.me_ref, bf16[768,2048]{1,0:T(8,128)(2,1)} %bitcast.29, bf16[2048,2048]{1,0:T(8,128)(2,1)} %key_ref.15, bf16[2048,2048]{1,0:T(8,128)(2,1)} %value_ref.15), custom_call_target="tpu_custom_call" | custom-call | flops 1476395008 | bytes 5701632 | tf_op jit(solution)/shard_map/project/pallas_call | solution.py:48
  42.7 1.9 %slice.49 = bf16[4,512,128]{2,1,0:T(8,128)(2,1)} slice(bf16[4,704,128]{2,1,0:T(8,128)(2,1)} %project.8.refs_7_), slice={[0:4], [0:512], [0:128]} | slice | bytes 1048576 | tf_op jit(solution)/shard_map/slice | solution.py:221
  44.6 1.6 slice.48
  47.9 4.1 %pad_maximum_fusion.tokens_ref = bf16[832,2048]{1,0:T(8,128)(2,1)} fusion(bf16[64,2048]{1,0:T(8,128)(2,1)S(1)} %collective-permute-done.3, bf16[768,2048]{1,0:T(8,128)(2,1)} %bitcast.30), kind=kLoop, calls=%fused_computation | loop fusion | flops 6815744 | bytes 6815744 | tf_op jit(solution)/shard_map/concatenate | solution.py:203
  52.0 5.1 %project.12.refs_3_ = bf16[4,832,128]{2,1,0:T(8,128)(2,1)} custom-call(s32[1]{0:T(128)} %bitcast.me_ref, bf16[832,2048]{1,0:T(8,128)(2,1)} %pad_maximum_fusion.tokens_ref, bf16[2048,2048]{1,0:T(8,128)(2,1)} %key_ref.15, bf16[2048,2048]{1,0:T(8,128)(2,1)} %value_ref.15), custom_call_target="tpu_custom_call" | custom-call | flops 1744830464 | bytes 6356992 | tf_op jit(solution)/shard_map/project/pallas_call | solution.py:48
  57.1 27.1 %collective-permute-start.6 = (bf16[4,832,128]{2,1,0:T(8,128)(2,1)}, bf16[4,832,128]{2,1,0:T(8,128)(2,1)S(1)}, u32[]{:S(2)}, u32[]{:S(2)}) collective-permute-start(bf16[4,832,128]{2,1,0:T(8,128)(2,1)} %project.12.refs_3_), channel_id=1, source_target_pairs={{0,4},{2,6},{4,0},{6,2},{8,12},{10,14},{12,8},{14,10},{1,5},{3,7},... | collective-permute-start | bytes 2555912 | tf_op jit(solution)/shard_map/ppermute | solution.py:197
  84.2 5.1 %project.10.refs_5_ = bf16[4,832,128]{2,1,0:T(8,128)(2,1)} custom-call(s32[1]{0:T(128)} %bitcast.me_ref, bf16[832,2048]{1,0:T(8,128)(2,1)} %pad_maximum_fusion.tokens_ref, bf16[2048,2048]{1,0:T(8,128)(2,1)} %key_ref.15, bf16[2048,2048]{1,0:T(8,128)(2,1)} %value_ref.15), custom_call_target="tpu_custom_call" | custom-call | flops 1744830464 | bytes 6356992 | tf_op jit(solution)/shard_map/project/pallas_call | solution.py:48
  89.3 5.1 %project.11.refs_4_ = bf16[4,832,128]{2,1,0:T(8,128)(2,1)} custom-call(s32[1]{0:T(128)} %bitcast.me_ref, bf16[832,2048]{1,0:T(8,128)(2,1)} %pad_maximum_fusion.tokens_ref, bf16[2048,2048]{1,0:T(8,128)(2,1)} %key_ref.15, bf16[2048,2048]{1,0:T(8,128)(2,1)} %value_ref.15), custom_call_target="tpu_custom_call" | custom-call | flops 1744830464 | bytes 6356992 | tf_op jit(solution)/shard_map/project/pallas_call | solution.py:48
  94.5 5.2 %project.15.block_ref.refs_0_ = bf16[4,832,128]{2,1,0:T(8,128)(2,1)} custom-call(s32[1]{0:T(128)} %bitcast.me_ref, bf16[832,2048]{1,0:T(8,128)(2,1)} %pad_maximum_fusion.tokens_ref, bf16[2048,2048]{1,0:T(8,128)(2,1)} %key_ref.15, bf16[2048,2048]{1,0:T(8,128)(2,1)} %value_ref.15), custom_call_target="tpu_custom_call" | custom-call | flops 1744830464 | bytes 6356992 | tf_op jit(solution)/shard_map/project/pallas_call | solution.py:48
  99.7 1.6 collective-permute-start.5
  101.2 13.1 %read.1 = f32[8,4,128]{2,1,0:T(4,128)} custom-call(s32[1]{0:T(128)} %bitcast.me_ref, f32[8,4,128]{2,1,0:T(4,128)} %pad_convert_fusion.query_ref, f32[8,4,768]{2,1,0:T(4,128)} %copy-done.3, f32[4,4,64]{2,1,0:T(4,128)} %copy-done.5, bf16[4,832,128]{2,1,0:T(8,128)(2,1)} %project.15.block_ref.refs_0_, bf16[4,704,128]{2,1,0:T(8,128)(2,1)} %project.14.refs_1_, ...), custom_call_target="tpu_custom_call" | custom-call | flops 50331648 | bytes 6291456 | tf_op jit(solution)/shard_map/read/pallas_call | solution.py:132
  114.4 4.0 %all-to-all-start.1 = ((f32[8,4,128]{2,1,0:T(4,128)}), f32[8,4,128]{2,1,0:T(4,128)S(1)}, u32[]{:S(2)}, u32[]{:S(2)}) async-start(f32[8,4,128]{2,1,0:T(4,128)} %read.1), calls=%async_computation.1 | async-start | bytes 32768 | tf_op jit(solution)/shard_map/all_to_all | solution.py:200
  119.2 2.9 %collective-permute-start.4 = (bf16[4,832,128]{2,1,0:T(8,128)(2,1)}, bf16[4,832,128]{2,1,0:T(8,128)(2,1)S(1)}, u32[]{:S(2)}, u32[]{:S(2)}) collective-permute-start(bf16[4,832,128]{2,1,0:T(8,128)(2,1)} %project.10.refs_5_), channel_id=1, source_target_pairs={{0,6},{2,4},{4,2},{6,0},{8,14},{10,12},{12,10},{14,8},{1,7},{3,5},... | collective-permute-start | bytes 2555912 | tf_op jit(solution)/shard_map/ppermute | solution.py:197
  122.2 1.6 slice_add_fusion
  124.7 29.0 %all-to-all-done.1 = f32[8,4,128]{2,1,0:T(4,128)S(1)} async-done(((f32[8,4,128]{2,1,0:T(4,128)}), f32[8,4,128]{2,1,0:T(4,128)S(1)}, u32[]{:S(2)}, u32[]{:S(2)}) %all-to-all-start.1) | async-done | bytes 16416 | tf_op jit(solution)/shard_map/all_to_all | solution.py:200
  153.7 1.8 %all_gather.3 = f32[16,4,128]{2,1,0:T(4,128)S(1)} all-gather(f32[8,4,128]{2,1,0:T(4,128)S(1)} %all-to-all-done.1), channel_id=1, replica_groups=mesh['gr'=2,'sp'=8,'tp'=2] {'tp'}, dimensions={0}, use_global_device_ids=true | all-gather | bytes 49152 | tf_op jit(solution)/shard_map/all_gather | solution.py:240
  156.6 1.1 copy-done.2
  158.7 2.0 %place.11.refs_0_ = bf16[4,6144,128]{2,1,0:T(8,128)(2,1)} custom-call(bf16[4,704,128]{2,1,0:T(8,128)(2,1)} %collective-permute-done.7.block_ref, bf16[4,6144,128]{2,1,0:T(8,128)(2,1)} %place.10.refs_0_), custom_call_target="tpu_custom_call", output_to_operand_aliasing={{}: (1, {})} | custom-call | flops 360448 | bytes 1441792 | tf_op jit(solution)/shard_map/place/pallas_call | solution.py:88
  160.8 3.4 %collective-permute-start = (bf16[4,192,128]{2,1,0:T(8,128)(2,1)S(1)}, bf16[4,192,128]{2,1,0:T(8,128)(2,1)S(1)}, u32[]{:S(2)}, u32[]{:S(2)}) collective-permute-start(bf16[4,192,128]{2,1,0:T(8,128)(2,1)S(1)} %copy-done.4), channel_id=1, source_target_pairs={{0,12},{2,14},{4,8},{6,10},{8,4},{10,6},{12,0},{14,2},{1,13},{3,15... | collective-permute-start | bytes 589832 | tf_op jit(solution)/shard_map/ppermute | solution.py:197
  165.8 0.9 place.13.refs_0_
  167.6 2.0 %place.15.refs_0_ = bf16[4,6144,128]{2,1,0:T(8,128)(2,1)} custom-call(bf16[4,704,128]{2,1,0:T(8,128)(2,1)} %collective-permute-done.2.block_ref, bf16[4,6144,128]{2,1,0:T(8,128)(2,1)} %place.14.refs_0_), custom_call_target="tpu_custom_call", output_to_operand_aliasing={{}: (1, {})} | custom-call | flops 360448 | bytes 1441792 | tf_op jit(solution)/shard_map/place/pallas_call | solution.py:88
  169.6 2.7 %collective-permute-done.1.block_ref = bf16[4,512,128]{2,1,0:T(8,128)(2,1)S(1)} collective-permute-done((bf16[4,512,128]{2,1,0:T(8,128)(2,1)}, bf16[4,512,128]{2,1,0:T(8,128)(2,1)S(1)}, u32[]{:S(2)}, u32[]{:S(2)}) %collective-permute-start.1) | collective-permute-done | bytes 524320 | tf_op jit(solution)/shard_map/ppermute | solution.py:197
  173.1 2.5 %collective-permute-done.block_ref = bf16[4,192,128]{2,1,0:T(8,128)(2,1)S(1)} collective-permute-done((bf16[4,192,128]{2,1,0:T(8,128)(2,1)S(1)}, bf16[4,192,128]{2,1,0:T(8,128)(2,1)S(1)}, u32[]{:S(2)}, u32[]{:S(2)}) %collective-permute-start) | collective-permute-done | bytes 196640 | tf_op jit(solution)/shard_map/ppermute | solution.py:197
  (56 shorter events, 11.6 us)
Async XLA Ops:
  1.8 19.0 %copy-start.3 = (f32[8,4,768]{2,1,0:T(4,128)}, f32[8,4,768]{2,1,0:T(4,128)S(1)}, u32[]{:S(2)}) copy-start(f32[8,4,768]{2,1,0:T(4,128)S(1)} %reshape_reshape_squeeze.5.gates_ref) | copy-start | bytes 294916
  3.8 42.4 %all-to-all-start = ((bf16[8,4,850]{2,1,0:T(4,128)(2,1)}), bf16[8,4,850]{2,1,0:T(4,128)(2,1)S(1)}, u32[]{:S(2)}, u32[]{:S(2)}) async-start(bf16[8,4,850]{2,1,0:T(4,128)(2,1)} %concatenate.7), calls=%async_computation | async-start | bytes 114688 | tf_op jit(solution)/shard_map/all_to_all | solution.py:200
  12.1 35.8 %collective-permute-start.3 = (bf16[64,2048]{1,0:T(8,128)(2,1)S(1)}, bf16[64,2048]{1,0:T(8,128)(2,1)S(1)}, u32[]{:S(2)}, u32[]{:S(2)}) collective-permute-start(bf16[64,2048]{1,0:T(8,128)(2,1)S(1)} %slice_bitcast_fusion), channel_id=1, source_target_pairs={{0,12},{2,14},{4,8},{6,10},{8,4},{10,6},{12,0},{14,2},{1,13},{3,15... | collective-permute-start | bytes 786440 | tf_op jit(solution)/shard_map/ppermute | solution.py:197
  16.0 83.6 %collective-permute-start.9 = (f32[4,4,64]{2,1,0:T(4,128)S(1)}, f32[4,4,64]{2,1,0:T(4,128)S(1)}, u32[]{:S(2)}, u32[]{:S(2)}) collective-permute-start(f32[4,4,64]{2,1,0:T(4,128)S(1)} %constant_dynamic-slice_fusion), channel_id=1, source_target_pairs={{0,12},{2,14},{4,8},{6,10},{8,4},{10,6},{12,0},{14,2},{1,13},{3,15... | collective-permute-start | bytes 12296 | tf_op jit(solution)/shard_map/ppermute | solution.py:197
  20.8 97.6 %collective-permute-start.8 = (bf16[4,704,128]{2,1,0:T(8,128)(2,1)}, bf16[4,704,128]{2,1,0:T(8,128)(2,1)S(1)}, u32[]{:S(2)}, u32[]{:S(2)}) collective-permute-start(bf16[4,704,128]{2,1,0:T(8,128)(2,1)} %project.14.refs_1_), channel_id=1, source_target_pairs={{0,14},{2,12},{4,10},{6,8},{8,6},{10,4},{12,2},{14,0},{1,15},{3,13... | collective-permute-start | bytes 2162696 | tf_op jit(solution)/shard_map/ppermute | solution.py:197
  30.2 125.3 %collective-permute-start.7 = (bf16[4,704,128]{2,1,0:T(8,128)(2,1)}, bf16[4,704,128]{2,1,0:T(8,128)(2,1)}, u32[]{:S(2)}, u32[]{:S(2)}) collective-permute-start(bf16[4,704,128]{2,1,0:T(8,128)(2,1)} %project.13.refs_2_), channel_id=1, source_target_pairs={{0,8},{2,10},{4,12},{6,14},{8,0},{10,2},{12,4},{14,6},{1,9},{3,11}... | collective-permute-start | bytes 2162696 | tf_op jit(solution)/shard_map/ppermute | solution.py:197
  35.0 132.6 %collective-permute-start.2 = (bf16[4,704,128]{2,1,0:T(8,128)(2,1)}, bf16[4,704,128]{2,1,0:T(8,128)(2,1)}, u32[]{:S(2)}, u32[]{:S(2)}) collective-permute-start(bf16[4,704,128]{2,1,0:T(8,128)(2,1)} %project.9.refs_6_), channel_id=1, source_target_pairs={{0,10},{2,8},{4,14},{6,12},{8,2},{10,0},{12,6},{14,4},{1,11},{3,9}... | collective-permute-start | bytes 2162696 | tf_op jit(solution)/shard_map/ppermute | solution.py:197
  57.1 103.6 %collective-permute-start.6 = (bf16[4,832,128]{2,1,0:T(8,128)(2,1)}, bf16[4,832,128]{2,1,0:T(8,128)(2,1)S(1)}, u32[]{:S(2)}, u32[]{:S(2)}) collective-permute-start(bf16[4,832,128]{2,1,0:T(8,128)(2,1)} %project.12.refs_3_), channel_id=1, source_target_pairs={{0,4},{2,6},{4,0},{6,2},{8,12},{10,14},{12,8},{14,10},{1,5},{3,7},... | collective-permute-start | bytes 2555912 | tf_op jit(solution)/shard_map/ppermute | solution.py:197
  99.6 24.1 %copy-start = (bf16[4,832,128]{2,1,0:T(8,128)(2,1)S(1)}, bf16[4,832,128]{2,1,0:T(8,128)(2,1)}, u32[]{:S(2)}) copy-start(bf16[4,832,128]{2,1,0:T(8,128)(2,1)} %project.15.block_ref.refs_0_) | copy-start | bytes 2555908
  99.7 1.6 copy-start.5
  99.7 66.1 %collective-permute-start.5 = (bf16[4,832,128]{2,1,0:T(8,128)(2,1)}, bf16[4,832,128]{2,1,0:T(8,128)(2,1)S(1)}, u32[]{:S(2)}, u32[]{:S(2)}) collective-permute-start(bf16[4,832,128]{2,1,0:T(8,128)(2,1)} %project.11.refs_4_), channel_id=1, source_target_pairs={{0,2},{2,0},{4,6},{6,4},{8,10},{10,8},{12,14},{14,12},{1,3},{3,1},... | collective-permute-start | bytes 2555912 | tf_op jit(solution)/shard_map/ppermute | solution.py:197
  114.4 39.3 %all-to-all-start.1 = ((f32[8,4,128]{2,1,0:T(4,128)}), f32[8,4,128]{2,1,0:T(4,128)S(1)}, u32[]{:S(2)}, u32[]{:S(2)}) async-start(f32[8,4,128]{2,1,0:T(4,128)} %read.1), calls=%async_computation.1 | async-start | bytes 32768 | tf_op jit(solution)/shard_map/all_to_all | solution.py:200
  118.4 0.9 copy-start.1
  119.2 47.4 %collective-permute-start.4 = (bf16[4,832,128]{2,1,0:T(8,128)(2,1)}, bf16[4,832,128]{2,1,0:T(8,128)(2,1)S(1)}, u32[]{:S(2)}, u32[]{:S(2)}) collective-permute-start(bf16[4,832,128]{2,1,0:T(8,128)(2,1)} %project.10.refs_5_), channel_id=1, source_target_pairs={{0,6},{2,4},{4,2},{6,0},{8,14},{10,12},{12,10},{14,8},{1,7},{3,5},... | collective-permute-start | bytes 2555912 | tf_op jit(solution)/shard_map/ppermute | solution.py:197
  155.5 16.9 %collective-permute-start.1 = (bf16[4,512,128]{2,1,0:T(8,128)(2,1)}, bf16[4,512,128]{2,1,0:T(8,128)(2,1)S(1)}, u32[]{:S(2)}, u32[]{:S(2)}) collective-permute-start(bf16[4,512,128]{2,1,0:T(8,128)(2,1)} %slice.49), channel_id=1, source_target_pairs={{0,12},{2,14},{4,8},{6,10},{8,4},{10,6},{12,0},{14,2},{1,13},{3,15... | collective-permute-start | bytes 1572872 | tf_op jit(solution)/shard_map/ppermute | solution.py:197
  156.6 1.1 copy-start.2
  158.7 2.0 %copy-start.4 = (bf16[4,192,128]{2,1,0:T(8,128)(2,1)S(1)}, bf16[4,192,128]{2,1,0:T(8,128)(2,1)}, u32[]{:S(2)}) copy-start(bf16[4,192,128]{2,1,0:T(8,128)(2,1)} %slice.48) | copy-start | bytes 589828
  160.8 14.9 %collective-permute-start = (bf16[4,192,128]{2,1,0:T(8,128)(2,1)S(1)}, bf16[4,192,128]{2,1,0:T(8,128)(2,1)S(1)}, u32[]{:S(2)}, u32[]{:S(2)}) collective-permute-start(bf16[4,192,128]{2,1,0:T(8,128)(2,1)S(1)} %copy-done.4), channel_id=1, source_target_pairs={{0,12},{2,14},{4,8},{6,10},{8,4},{10,6},{12,0},{14,2},{1,13},{3,15... | collective-permute-start | bytes 589832 | tf_op jit(solution)/shard_map/ppermute | solution.py:197

commit v3 on v2

--- a/solution.py
+++ b/solution.py
@@ -9,7 +9,7 @@
 
 LANES = 128
 ROWS = 64
-TAIL = 192
+TAIL = 128
 MIB = 1 << 20
 
 
@@ -230,7 +230,8 @@
     queries = told[:, :, -size:]
     gate_parts = unpacked_gates(told[:, :, :-size], length)
     gate_cache = jnp.transpose(gate_parts, (1, 0, 2)).reshape(1, heads, places * length)
-    borrowed = swap(lax.dynamic_slice(gates, ((me ^ far) & far, 0, kept), (far, heads, ROWS)), peer)
+    borrowed = lax.dynamic_slice(gates, ((me ^ far) & far, 0, kept), (far, heads, ROWS))
+    borrowed = swap(borrowed.reshape(-1, LANES), peer).reshape(borrowed.shape)
 
     sent[0] = block_of(0)
     cache = place(None, sent[0], parts_of(0), places, length)

time: 177 us -> 176 us (level)
  waiting for transfers between devices: 34.3 us -> 30.9 us
    all_to_all x2, waiting for transfers between devices: 29 us -> 11.8 us  [exchange(): return lax.all_to_all(value, 'sp', split_axis=0, concat_axis=0, tiled=True)]
    ppermute x10, waiting for transfers between devices: 5.28 us -> 19.1 us  [swap(): return lax.ppermute(value, 'sp', [(i, i ^ step) for i in range(places)])]
  transfers between devices with their start and end apart: 12 -> 12, of which waited for: 3 -> 2; matrix products, arithmetic and copies ran while one was open for 8% -> 8% of each run, Pallas kernels for 35% -> 35%
where the time goes in v3:
time: 176 us; the launch traced here: 175 us
  Pallas kernels  62.7 us (36%)
  starting transfers between devices  59.9 us (34%)
  waiting for transfers between devices  30.9 us (18%)
  local copies, waits for them, and re-layouts  10.5 us (6%)
  other arithmetic  8.57 us (5%)
  blocking collectives  1.82 us (1%)
    ppermute x10, starting transfers between devices, swap(): return lax.ppermute(value, 'sp', [(i, i ^ step) for i in range(places)])  48.6 us
    pallas_call x8, Pallas kernels, project(): pl.pallas_call(functools.partial(project_block, step), grid_spec=pltpu.Pr...  39.5 us
    ppermute x10, waiting for transfers between devices, swap(): return lax.ppermute(value, 'sp', [(i, i ^ step) for i in range(places)])  19.1 us
    pallas_call x1, Pallas kernels, partial_reads(): pl.pallas_call(functools.partial(read_blocks, steps, near), in_specs=[pl....  13.2 us
    all_to_all x2, waiting for transfers between devices, exchange(): return lax.all_to_all(value, 'sp', split_axis=0, concat_axis=0, tiled=True)  11.8 us
    all_to_all x2, starting transfers between devices, exchange(): return lax.all_to_all(value, 'sp', split_axis=0, concat_axis=0, tiled=True)  11.3 us
    pallas_call x9, Pallas kernels, place(): pl.pallas_call(functools.partial(place_block, parts, length), in_specs=[p...  10 us
    concatenate x1, other arithmetic, on_device(): more = jnp.concatenate([rows, lent], axis=0)  4.09 us
  transfers between devices with their start and end apart: 12, of which 2 were waited for; matrix products, arithmetic and copies ran while one was open for 8% of the time, Pallas kernels for 35%

profile of v3, /device:TPU:0, one launch (start us, length us, event | category | flops | bytes accessed | tf_op | source)
XLA Modules:
  0.0 175.3 jit_solution(3428007701998152525)
XLA Ops:
  0.6 1.1 reduce.2
  3.8 7.3 %all-to-all-start = ((bf16[8,4,850]{2,1,0:T(4,128)(2,1)}), bf16[8,4,850]{2,1,0:T(4,128)(2,1)S(1)}, u32[]{:S(2)}, u32[]{:S(2)}) async-start(bf16[8,4,850]{2,1,0:T(4,128)(2,1)} %concatenate.7), calls=%async_computation | async-start | bytes 114688 | tf_op jit(solution)/shard_map/all_to_all | solution.py:200
  11.1 1.0 slice_bitcast_fusion
  12.1 3.9 %collective-permute-start.3 = (bf16[64,2048]{1,0:T(8,128)(2,1)S(1)}, bf16[64,2048]{1,0:T(8,128)(2,1)S(1)}, u32[]{:S(2)}, u32[]{:S(2)}) collective-permute-start(bf16[64,2048]{1,0:T(8,128)(2,1)S(1)} %slice_bitcast_fusion), channel_id=1, source_target_pairs={{0,12},{2,14},{4,8},{6,10},{8,4},{10,6},{12,0},{14,2},{1,13},{3,15... | collective-permute-start | bytes 786440 | tf_op jit(solution)/shard_map/ppermute | solution.py:197
  16.1 4.7 %project.14.refs_1_ = bf16[4,704,128]{2,1,0:T(8,128)(2,1)} custom-call(s32[1]{0:T(128)} %bitcast.me_ref, bf16[768,2048]{1,0:T(8,128)(2,1)} %bitcast.26, bf16[2048,2048]{1,0:T(8,128)(2,1)} %key_ref.15, bf16[2048,2048]{1,0:T(8,128)(2,1)} %value_ref.15), custom_call_target="tpu_custom_call" | custom-call | flops 1476395008 | bytes 5701632 | tf_op jit(solution)/shard_map/project/pallas_call | solution.py:48
  20.9 4.7 %collective-permute-start.8 = (bf16[4,704,128]{2,1,0:T(8,128)(2,1)}, bf16[4,704,128]{2,1,0:T(8,128)(2,1)S(1)}, u32[]{:S(2)}, u32[]{:S(2)}) collective-permute-start(bf16[4,704,128]{2,1,0:T(8,128)(2,1)} %project.14.refs_1_), channel_id=1, source_target_pairs={{0,14},{2,12},{4,10},{6,8},{8,6},{10,4},{12,2},{14,0},{1,15},{3,13... | collective-permute-start | bytes 2162696 | tf_op jit(solution)/shard_map/ppermute | solution.py:197
  25.6 4.8 %project.13.refs_2_ = bf16[4,704,128]{2,1,0:T(8,128)(2,1)} custom-call(s32[1]{0:T(128)} %bitcast.me_ref, bf16[768,2048]{1,0:T(8,128)(2,1)} %bitcast.27, bf16[2048,2048]{1,0:T(8,128)(2,1)} %key_ref.15, bf16[2048,2048]{1,0:T(8,128)(2,1)} %value_ref.15), custom_call_target="tpu_custom_call" | custom-call | flops 1476395008 | bytes 5701632 | tf_op jit(solution)/shard_map/project/pallas_call | solution.py:48
  30.3 4.8 %project.9.refs_6_ = bf16[4,704,128]{2,1,0:T(8,128)(2,1)} custom-call(s32[1]{0:T(128)} %bitcast.me_ref, bf16[768,2048]{1,0:T(8,128)(2,1)} %bitcast.28, bf16[2048,2048]{1,0:T(8,128)(2,1)} %key_ref.15, bf16[2048,2048]{1,0:T(8,128)(2,1)} %value_ref.15), custom_call_target="tpu_custom_call" | custom-call | flops 1476395008 | bytes 5701632 | tf_op jit(solution)/shard_map/project/pallas_call | solution.py:48
  35.1 2.9 %collective-permute-start.2 = (bf16[4,704,128]{2,1,0:T(8,128)(2,1)}, bf16[4,704,128]{2,1,0:T(8,128)(2,1)}, u32[]{:S(2)}, u32[]{:S(2)}) collective-permute-start(bf16[4,704,128]{2,1,0:T(8,128)(2,1)} %project.9.refs_6_), channel_id=1, source_target_pairs={{0,10},{2,8},{4,14},{6,12},{8,2},{10,0},{12,6},{14,4},{1,11},{3,9}... | collective-permute-start | bytes 2162696 | tf_op jit(solution)/shard_map/ppermute | solution.py:197
  38.0 4.8 %project.8.refs_7_ = bf16[4,704,128]{2,1,0:T(8,128)(2,1)} custom-call(s32[1]{0:T(128)} %bitcast.me_ref, bf16[768,2048]{1,0:T(8,128)(2,1)} %bitcast.29, bf16[2048,2048]{1,0:T(8,128)(2,1)} %key_ref.15, bf16[2048,2048]{1,0:T(8,128)(2,1)} %value_ref.15), custom_call_target="tpu_custom_call" | custom-call | flops 1476395008 | bytes 5701632 | tf_op jit(solution)/shard_map/project/pallas_call | solution.py:48
  42.8 2.0 %slice.49 = bf16[4,576,128]{2,1,0:T(8,128)(2,1)} slice(bf16[4,704,128]{2,1,0:T(8,128)(2,1)} %project.8.refs_7_), slice={[0:4], [0:576], [0:128]} | slice | bytes 1179648 | tf_op jit(solution)/shard_map/slice | solution.py:221
  44.8 1.6 slice.48
  48.7 4.1 %pad_maximum_fusion.tokens_ref = bf16[832,2048]{1,0:T(8,128)(2,1)} fusion(bf16[64,2048]{1,0:T(8,128)(2,1)S(1)} %collective-permute-done.3, bf16[768,2048]{1,0:T(8,128)(2,1)} %bitcast.30), kind=kLoop, calls=%fused_computation | loop fusion | flops 6815744 | bytes 6815744 | tf_op jit(solution)/shard_map/concatenate | solution.py:203
  52.8 5.1 %project.12.refs_3_ = bf16[4,832,128]{2,1,0:T(8,128)(2,1)} custom-call(s32[1]{0:T(128)} %bitcast.me_ref, bf16[832,2048]{1,0:T(8,128)(2,1)} %pad_maximum_fusion.tokens_ref, bf16[2048,2048]{1,0:T(8,128)(2,1)} %key_ref.15, bf16[2048,2048]{1,0:T(8,128)(2,1)} %value_ref.15), custom_call_target="tpu_custom_call" | custom-call | flops 1744830464 | bytes 6356992 | tf_op jit(solution)/shard_map/project/pallas_call | solution.py:48
  57.9 28.7 %collective-permute-start.6 = (bf16[4,832,128]{2,1,0:T(8,128)(2,1)}, bf16[4,832,128]{2,1,0:T(8,128)(2,1)S(1)}, u32[]{:S(2)}, u32[]{:S(2)}) collective-permute-start(bf16[4,832,128]{2,1,0:T(8,128)(2,1)} %project.12.refs_3_), channel_id=1, source_target_pairs={{0,4},{2,6},{4,0},{6,2},{8,12},{10,14},{12,8},{14,10},{1,5},{3,7},... | collective-permute-start | bytes 2555912 | tf_op jit(solution)/shard_map/ppermute | solution.py:197
  86.6 5.1 %project.11.refs_4_ = bf16[4,832,128]{2,1,0:T(8,128)(2,1)} custom-call(s32[1]{0:T(128)} %bitcast.me_ref, bf16[832,2048]{1,0:T(8,128)(2,1)} %pad_maximum_fusion.tokens_ref, bf16[2048,2048]{1,0:T(8,128)(2,1)} %key_ref.15, bf16[2048,2048]{1,0:T(8,128)(2,1)} %value_ref.15), custom_call_target="tpu_custom_call" | custom-call | flops 1744830464 | bytes 6356992 | tf_op jit(solution)/shard_map/project/pallas_call | solution.py:48
  91.8 1.5 collective-permute-start.5
  93.3 5.1 %project.10.refs_5_ = bf16[4,832,128]{2,1,0:T(8,128)(2,1)} custom-call(s32[1]{0:T(128)} %bitcast.me_ref, bf16[832,2048]{1,0:T(8,128)(2,1)} %pad_maximum_fusion.tokens_ref, bf16[2048,2048]{1,0:T(8,128)(2,1)} %key_ref.15, bf16[2048,2048]{1,0:T(8,128)(2,1)} %value_ref.15), custom_call_target="tpu_custom_call" | custom-call | flops 1744830464 | bytes 6356992 | tf_op jit(solution)/shard_map/project/pallas_call | solution.py:48
  98.4 5.1 %project.15.block_ref.refs_0_ = bf16[4,832,128]{2,1,0:T(8,128)(2,1)} custom-call(s32[1]{0:T(128)} %bitcast.me_ref, bf16[832,2048]{1,0:T(8,128)(2,1)} %pad_maximum_fusion.tokens_ref, bf16[2048,2048]{1,0:T(8,128)(2,1)} %key_ref.15, bf16[2048,2048]{1,0:T(8,128)(2,1)} %value_ref.15), custom_call_target="tpu_custom_call" | custom-call | flops 1744830464 | bytes 6356992 | tf_op jit(solution)/shard_map/project/pallas_call | solution.py:48
  103.5 13.2 %read.1 = f32[8,4,128]{2,1,0:T(4,128)} custom-call(s32[1]{0:T(128)} %bitcast.me_ref, f32[8,4,128]{2,1,0:T(4,128)} %pad_convert_fusion.query_ref, f32[8,4,768]{2,1,0:T(4,128)} %copy-done.3, f32[4,4,64]{2,1,0:T(4,128)} %reshape.65.borrowed_ref, bf16[4,832,128]{2,1,0:T(8,128)(2,1)} %project.15.block_ref.refs_0_, bf16[4,704,128]{2,1,0:T(8,128)(2,1)} %project.14.refs_1_, ...), custom_call_target="tpu_custom_call" | custom-call | flops 50331648 | bytes 6291456 | tf_op jit(solution)/shard_map/read/pallas_call | solution.py:132
  116.7 4.0 %all-to-all-start.1 = ((f32[8,4,128]{2,1,0:T(4,128)}), f32[8,4,128]{2,1,0:T(4,128)S(1)}, u32[]{:S(2)}, u32[]{:S(2)}) async-start(f32[8,4,128]{2,1,0:T(4,128)} %read.1), calls=%async_computation.1 | async-start | bytes 32768 | tf_op jit(solution)/shard_map/all_to_all | solution.py:200
  121.6 2.9 %collective-permute-start.4 = (bf16[4,832,128]{2,1,0:T(8,128)(2,1)}, bf16[4,832,128]{2,1,0:T(8,128)(2,1)S(1)}, u32[]{:S(2)}, u32[]{:S(2)}) collective-permute-start(bf16[4,832,128]{2,1,0:T(8,128)(2,1)} %project.10.refs_5_), channel_id=1, source_target_pairs={{0,6},{2,4},{4,2},{6,0},{8,14},{10,12},{12,10},{14,8},{1,7},{3,5},... | collective-permute-start | bytes 2555912 | tf_op jit(solution)/shard_map/ppermute | solution.py:197
  124.5 1.6 slice_add_fusion
  127.0 11.8 %all-to-all-done.1 = f32[8,4,128]{2,1,0:T(4,128)S(1)} async-done(((f32[8,4,128]{2,1,0:T(4,128)}), f32[8,4,128]{2,1,0:T(4,128)S(1)}, u32[]{:S(2)}, u32[]{:S(2)}) %all-to-all-start.1) | async-done | bytes 16416 | tf_op jit(solution)/shard_map/all_to_all | solution.py:200
  138.7 1.8 %all_gather.3 = f32[16,4,128]{2,1,0:T(4,128)S(1)} all-gather(f32[8,4,128]{2,1,0:T(4,128)S(1)} %all-to-all-done.1), channel_id=1, replica_groups=mesh['gr'=2,'sp'=8,'tp'=2] {'tp'}, dimensions={0}, use_global_device_ids=true | all-gather | bytes 49152 | tf_op jit(solution)/shard_map/all_gather | solution.py:241
  140.6 1.9 %collective-permute-start.1 = (bf16[4,576,128]{2,1,0:T(8,128)(2,1)}, bf16[4,576,128]{2,1,0:T(8,128)(2,1)S(1)}, u32[]{:S(2)}, u32[]{:S(2)}) collective-permute-start(bf16[4,576,128]{2,1,0:T(8,128)(2,1)} %slice.49), channel_id=1, source_target_pairs={{0,12},{2,14},{4,8},{6,10},{8,4},{10,6},{12,0},{14,2},{1,13},{3,15... | collective-permute-start | bytes 1769480 | tf_op jit(solution)/shard_map/ppermute | solution.py:197
  143.1 1.1 copy-done.2
  145.2 2.0 %place.11.refs_0_ = bf16[4,6144,128]{2,1,0:T(8,128)(2,1)} custom-call(bf16[4,704,128]{2,1,0:T(8,128)(2,1)} %collective-permute-done.7.block_ref, bf16[4,6144,128]{2,1,0:T(8,128)(2,1)} %place.10.refs_0_), custom_call_target="tpu_custom_call", output_to_operand_aliasing={{}: (1, {})} | custom-call | flops 360448 | bytes 1441792 | tf_op jit(solution)/shard_map/place/pallas_call | solution.py:88
  147.2 2.0 %collective-permute-start = (bf16[4,128,128]{2,1,0:T(8,128)(2,1)S(1)}, bf16[4,128,128]{2,1,0:T(8,128)(2,1)S(1)}, u32[]{:S(2)}, u32[]{:S(2)}) collective-permute-start(bf16[4,128,128]{2,1,0:T(8,128)(2,1)S(1)} %copy-done.4), channel_id=1, source_target_pairs={{0,12},{2,14},{4,8},{6,10},{8,4},{10,6},{12,0},{14,2},{1,13},{3,15... | collective-permute-start | bytes 393224 | tf_op jit(solution)/shard_map/ppermute | solution.py:197
  150.8 0.9 place.13.refs_0_
  151.8 19.1 %collective-permute-done.4.block_ref = bf16[4,832,128]{2,1,0:T(8,128)(2,1)S(1)} collective-permute-done((bf16[4,832,128]{2,1,0:T(8,128)(2,1)}, bf16[4,832,128]{2,1,0:T(8,128)(2,1)S(1)}, u32[]{:S(2)}, u32[]{:S(2)}) %collective-permute-start.4) | collective-permute-done | bytes 852000 | tf_op jit(solution)/shard_map/ppermute | solution.py:197
  171.8 2.0 %place.15.refs_0_ = bf16[4,6144,128]{2,1,0:T(8,128)(2,1)} custom-call(bf16[4,704,128]{2,1,0:T(8,128)(2,1)} %collective-permute-done.2.block_ref, bf16[4,6144,128]{2,1,0:T(8,128)(2,1)} %place.14.refs_0_), custom_call_target="tpu_custom_call", output_to_operand_aliasing={{}: (1, {})} | custom-call | flops 360448 | bytes 1441792 | tf_op jit(solution)/shard_map/place/pallas_call | solution.py:88
  (56 shorter events, 11.8 us)
Async XLA Ops:
  1.8 19.1 %copy-start.3 = (f32[8,4,768]{2,1,0:T(4,128)}, f32[8,4,768]{2,1,0:T(4,128)S(1)}, u32[]{:S(2)}) copy-start(f32[8,4,768]{2,1,0:T(4,128)S(1)} %reshape_reshape_squeeze.5.gates_ref) | copy-start | bytes 294916
  3.8 43.2 %all-to-all-start = ((bf16[8,4,850]{2,1,0:T(4,128)(2,1)}), bf16[8,4,850]{2,1,0:T(4,128)(2,1)S(1)}, u32[]{:S(2)}, u32[]{:S(2)}) async-start(bf16[8,4,850]{2,1,0:T(4,128)(2,1)} %concatenate.7), calls=%async_computation | async-start | bytes 114688 | tf_op jit(solution)/shard_map/all_to_all | solution.py:200
  12.1 36.7 %collective-permute-start.3 = (bf16[64,2048]{1,0:T(8,128)(2,1)S(1)}, bf16[64,2048]{1,0:T(8,128)(2,1)S(1)}, u32[]{:S(2)}, u32[]{:S(2)}) collective-permute-start(bf16[64,2048]{1,0:T(8,128)(2,1)S(1)} %slice_bitcast_fusion), channel_id=1, source_target_pairs={{0,12},{2,14},{4,8},{6,10},{8,4},{10,6},{12,0},{14,2},{1,13},{3,15... | collective-permute-start | bytes 786440 | tf_op jit(solution)/shard_map/ppermute | solution.py:197
  16.1 30.2 %collective-permute-start.9 = (f32[8,128]{1,0:T(8,128)S(1)}, f32[8,128]{1,0:T(8,128)S(1)}, u32[]{:S(2)}, u32[]{:S(2)}) collective-permute-start(f32[8,128]{1,0:T(8,128)S(1)} %reshape.64), channel_id=1, source_target_pairs={{0,12},{2,14},{4,8},{6,10},{8,4},{10,6},{12,0},{14,2},{1,13},{3,15... | collective-permute-start | bytes 12296 | tf_op jit(solution)/shard_map/ppermute | solution.py:197
  20.9 99.8 %collective-permute-start.8 = (bf16[4,704,128]{2,1,0:T(8,128)(2,1)}, bf16[4,704,128]{2,1,0:T(8,128)(2,1)S(1)}, u32[]{:S(2)}, u32[]{:S(2)}) collective-permute-start(bf16[4,704,128]{2,1,0:T(8,128)(2,1)} %project.14.refs_1_), channel_id=1, source_target_pairs={{0,14},{2,12},{4,10},{6,8},{8,6},{10,4},{12,2},{14,0},{1,15},{3,13... | collective-permute-start | bytes 2162696 | tf_op jit(solution)/shard_map/ppermute | solution.py:197
  30.3 110.2 %collective-permute-start.7 = (bf16[4,704,128]{2,1,0:T(8,128)(2,1)}, bf16[4,704,128]{2,1,0:T(8,128)(2,1)}, u32[]{:S(2)}, u32[]{:S(2)}) collective-permute-start(bf16[4,704,128]{2,1,0:T(8,128)(2,1)} %project.13.refs_2_), channel_id=1, source_target_pairs={{0,8},{2,10},{4,12},{6,14},{8,0},{10,2},{12,4},{14,6},{1,9},{3,11}... | collective-permute-start | bytes 2162696 | tf_op jit(solution)/shard_map/ppermute | solution.py:197
  35.1 136.6 %collective-permute-start.2 = (bf16[4,704,128]{2,1,0:T(8,128)(2,1)}, bf16[4,704,128]{2,1,0:T(8,128)(2,1)}, u32[]{:S(2)}, u32[]{:S(2)}) collective-permute-start(bf16[4,704,128]{2,1,0:T(8,128)(2,1)} %project.9.refs_6_), channel_id=1, source_target_pairs={{0,10},{2,8},{4,14},{6,12},{8,2},{10,0},{12,6},{14,4},{1,11},{3,9}... | collective-permute-start | bytes 2162696 | tf_op jit(solution)/shard_map/ppermute | solution.py:197
  57.9 89.3 %collective-permute-start.6 = (bf16[4,832,128]{2,1,0:T(8,128)(2,1)}, bf16[4,832,128]{2,1,0:T(8,128)(2,1)S(1)}, u32[]{:S(2)}, u32[]{:S(2)}) collective-permute-start(bf16[4,832,128]{2,1,0:T(8,128)(2,1)} %project.12.refs_3_), channel_id=1, source_target_pairs={{0,4},{2,6},{4,0},{6,2},{8,12},{10,14},{12,8},{14,10},{1,5},{3,7},... | collective-permute-start | bytes 2555912 | tf_op jit(solution)/shard_map/ppermute | solution.py:197
  91.8 59.1 %collective-permute-start.5 = (bf16[4,832,128]{2,1,0:T(8,128)(2,1)}, bf16[4,832,128]{2,1,0:T(8,128)(2,1)S(1)}, u32[]{:S(2)}, u32[]{:S(2)}) collective-permute-start(bf16[4,832,128]{2,1,0:T(8,128)(2,1)} %project.11.refs_4_), channel_id=1, source_target_pairs={{0,2},{2,0},{4,6},{6,4},{8,10},{10,8},{12,14},{14,12},{1,3},{3,1},... | collective-permute-start | bytes 2555912 | tf_op jit(solution)/shard_map/ppermute | solution.py:197
  103.5 22.6 %copy-start = (bf16[4,832,128]{2,1,0:T(8,128)(2,1)S(1)}, bf16[4,832,128]{2,1,0:T(8,128)(2,1)}, u32[]{:S(2)}) copy-start(bf16[4,832,128]{2,1,0:T(8,128)(2,1)} %project.15.block_ref.refs_0_) | copy-start | bytes 2555908
  116.7 22.1 %all-to-all-start.1 = ((f32[8,4,128]{2,1,0:T(4,128)}), f32[8,4,128]{2,1,0:T(4,128)S(1)}, u32[]{:S(2)}, u32[]{:S(2)}) async-start(f32[8,4,128]{2,1,0:T(4,128)} %read.1), calls=%async_computation.1 | async-start | bytes 32768 | tf_op jit(solution)/shard_map/all_to_all | solution.py:200
  120.7 0.9 copy-start.1
  121.6 49.3 %collective-permute-start.4 = (bf16[4,832,128]{2,1,0:T(8,128)(2,1)}, bf16[4,832,128]{2,1,0:T(8,128)(2,1)S(1)}, u32[]{:S(2)}, u32[]{:S(2)}) collective-permute-start(bf16[4,832,128]{2,1,0:T(8,128)(2,1)} %project.10.refs_5_), channel_id=1, source_target_pairs={{0,6},{2,4},{4,2},{6,0},{8,14},{10,12},{12,10},{14,8},{1,7},{3,5},... | collective-permute-start | bytes 2555912 | tf_op jit(solution)/shard_map/ppermute | solution.py:197
  140.6 33.2 %collective-permute-start.1 = (bf16[4,576,128]{2,1,0:T(8,128)(2,1)}, bf16[4,576,128]{2,1,0:T(8,128)(2,1)S(1)}, u32[]{:S(2)}, u32[]{:S(2)}) collective-permute-start(bf16[4,576,128]{2,1,0:T(8,128)(2,1)} %slice.49), channel_id=1, source_target_pairs={{0,12},{2,14},{4,8},{6,10},{8,4},{10,6},{12,0},{14,2},{1,13},{3,15... | collective-permute-start | bytes 1769480 | tf_op jit(solution)/shard_map/ppermute | solution.py:197
  143.1 1.1 copy-start.2
  145.2 2.0 %copy-start.4 = (bf16[4,128,128]{2,1,0:T(8,128)(2,1)S(1)}, bf16[4,128,128]{2,1,0:T(8,128)(2,1)}, u32[]{:S(2)}) copy-start(bf16[4,128,128]{2,1,0:T(8,128)(2,1)} %slice.48) | copy-start | bytes 393220
  147.2 27.4 %collective-permute-start = (bf16[4,128,128]{2,1,0:T(8,128)(2,1)S(1)}, bf16[4,128,128]{2,1,0:T(8,128)(2,1)S(1)}, u32[]{:S(2)}, u32[]{:S(2)}) collective-permute-start(bf16[4,128,128]{2,1,0:T(8,128)(2,1)S(1)} %copy-done.4), channel_id=1, source_target_pairs={{0,12},{2,14},{4,8},{6,10},{8,4},{10,6},{12,0},{14,2},{1,13},{3,15... | collective-permute-start | bytes 393224 | tf_op jit(solution)/shard_map/ppermute | solution.py:197
